TPU v7x, 512 devices: a whole 4x8x8 slice. The times are simulated.
512 devices in a mesh: sp: 64 (over z, y), tp: 8 (over x, core).
Axes of the slice: x: 4, y: 8, z: 8, core: 2. Of those that a mesh axis runs over, the one named last changes fastest.
Arguments:
- tokens: bfloat16 [16384, 2048], P('sp', 'tp'), may hold values from -24 to 24
- value_weight: bfloat16 [2, 2048, 2048], P(None, 'sp', 'tp'), may hold values from -0.125 to 0.125
- outer_weight: bfloat16 [2, 2048, 2048], P(None, 'sp', 'tp'), may hold values from -0.125 to 0.125
- inner_weight: bfloat16 [2, 2048, 2048], P(None, 'sp', 'tp'), may hold values from -0.125 to 0.125
- conv_taps: float32 [2, 3, 2048], P(None, None, 'tp'), may hold values from -3.5 to 3.5
- output_weight: bfloat16 [2, 2048, 2048], P(None, 'tp', 'sp'), may hold values from -2 to 2
- norm_gain: float32 [2, 2048], P(None, 'tp'), may hold values from 0.1 to 1.9
- norm_bias: float32 [2, 2048], P(None, 'tp'), may hold values from -3 to 3
Outputs:
- mixed_out: bfloat16 [16384, 2048], P('sp', 'tp')
All inputs are finite; a program needn't handle non-finite values.
Results may differ from a plain program's by a relative error of at most 0.03.
Values may be sent and summed in bfloat16 or wider, within the bound.
No kernel may reach another device: no remote copies, remote signals or barrier semaphores. Data moves between devices by JAX's collectives and lax.ppermute only.
A program may use at most 64 MiB of HBM per device.

v0:
```python
import jax
import jax.numpy as jnp
from jax import lax
from jax.sharding import PartitionSpec as P

D = 2048
LAYERS = 2


def gather_turned(arrays, axis, dims):
    turned = [jnp.moveaxis(a, dim, 0) for a, dim in zip(arrays, dims)]
    both = jnp.concatenate([t.reshape(len(t), -1) for t in turned], axis=1)
    whole, at, finished = (lax.all_gather(both, axis, axis=0, tiled=True), 0, [])
    for t, dim in zip(turned, dims):
        share = whole[:, at : at + t[0].size].reshape(-1, *t.shape[1:])
        finished.append(jnp.moveaxis(share, 0, dim))
        at += t[0].size
    return tuple(finished)


def laid_out(tiles, dim):
    tiles = jnp.moveaxis(tiles, 0, dim)
    shape = tiles.shape
    return tiles.reshape(*shape[:dim], shape[dim] * shape[dim + 1], *shape[dim + 2 :])


def sent_to_all(array, axis):
    peers = lax.axis_size(axis)
    return lax.all_to_all(
        jnp.broadcast_to(array[None], (peers, *array.shape)), axis, 0, 0, tiled=True
    )


def gather_directly(array, axis, dim):
    return laid_out(sent_to_all(array, axis), dim)


def from_behind(array, axis, by):
    peers = lax.axis_size(axis)
    pairs = [(i, i + by) for i in range(peers) if 0 <= i + by < peers]
    return lax.ppermute(array, axis, pairs)


def in_blocks(array, dim, peers):
    shape = array.shape
    tiles = array.reshape(*shape[:dim], peers, shape[dim] // peers, *shape[dim + 1 :])
    return jnp.moveaxis(tiles, dim, 0)


def summed_on_arrival(array, axis, dim):
    peers = lax.axis_size(axis)
    tiles = lax.all_to_all(in_blocks(array, dim, peers), axis, 0, 0, tiled=True)
    return jnp.sum(tiles.astype(jnp.float32), axis=0)


def of_everyone(array, axis):
    return sent_to_all(array, axis).sum(axis=0)


def packed_total(arrays, axis):
    ends = [0]
    for a in arrays:
        ends.append(ends[-1] + a.size)
    running = of_everyone(jnp.concatenate([a.ravel() for a in arrays]), axis)
    return tuple((running[b:e].reshape(a.shape) for a, b, e in zip(arrays, ends, ends[1:])))


def input_products(whole, weights):
    return tuple(
        (
            jnp.dot(whole, weight, preferred_element_type=jnp.float32).astype(jnp.bfloat16)
            for weight in weights
        )
    )


def shards(
    tokens, value_weight, outer_weight, inner_weight, conv_taps, output_weight, norm_gain, norm_bias
):
    alpha = (2.0 * LAYERS) ** 0.25
    state = tokens
    taps_count = conv_taps.shape[1]
    all_value, all_outer, all_inner, all_output = gather_turned(
        (value_weight, outer_weight, inner_weight, output_weight), "sp", (1, 1, 1, 2)
    )
    for layer in range(LAYERS):
        whole = gather_directly(state, "tp", 1)
        u_part, outer, inner = input_products(
            whole, (all_value[layer], all_outer[layer], all_inner[layer])
        )
        gated_in = inner.astype(jnp.float32) * u_part.astype(jnp.float32)
        previous = from_behind(gated_in[gated_in.shape[0] - (taps_count - 1) :], "sp", 1)
        padded = jnp.concatenate([previous, gated_in], axis=0)
        conv = jnp.zeros_like(gated_in)
        for tap in range(taps_count):
            conv = conv + conv_taps[layer, tap][None, :] * padded[tap : tap + gated_in.shape[0]]
        gated = (outer.astype(jnp.float32) * conv).astype(jnp.bfloat16)
        terms = jnp.dot(gated, all_output[layer], preferred_element_type=jnp.float32)
        branch = summed_on_arrival(terms.astype(jnp.bfloat16), "tp", 1)
        pre = alpha * state.astype(jnp.float32) + branch
        total, squares = packed_total(
            (jnp.sum(pre, axis=-1, keepdims=True), jnp.sum(pre * pre, axis=-1, keepdims=True)), "tp"
        )
        mean = total / D
        var = jnp.maximum(squares / D - mean * mean, 0.0)
        normed = (pre - mean) * lax.rsqrt(var + 1e-05)
        state = (normed * norm_gain[layer][None, :] + norm_bias[layer][None, :]).astype(
            jnp.bfloat16
        )
    return state


def solution(mesh):
    in_specs = (
        P("sp", "tp"),
        P(None, "sp", "tp"),
        P(None, "sp", "tp"),
        P(None, "sp", "tp"),
        P(None, None, "tp"),
        P(None, "tp", "sp"),
        P(None, "tp"),
        P(None, "tp"),
    )
    out_specs = P("sp", "tp")
    return jax.shard_map(shards, mesh=mesh, in_specs=in_specs, out_specs=out_specs, check_vma=False)
```

profile of v0, /device:TPU:1, one launch (start us, length us, event | category | flops | bytes accessed | tf_op | source)
XLA Modules:
  0.0 233.8 jit_solution(11278875935599742421)
XLA Ops:
  6.5 0.8 copy.77
  7.3 0.8 copy.78
  8.1 0.8 copy.79
  8.8 0.8 copy.80
  9.6 0.7 pad_maximum_fusion.2
  10.3 1.0 copy.52
  11.3 1.1 broadcast_in_dim.8
  12.4 10.3 %all-to-all-start = ((bf16[8,256,256]{1,2,0:T(8,128)(2,1)}), bf16[8,256,256]{1,2,0:T(8,128)(2,1)S(1)}, u32[]{:S(2)}, u32[]{:S(2)}) async-start(bf16[8,256,256]{1,2,0:T(8,128)(2,1)} %broadcast_in_dim.8), calls=%async_computation | async-start | bytes 2097152 | tf_op jit(solution)/shard_map/all_to_all | solution.py:29
  22.7 92.1 %all-gather.2.cloned.1.call-done = bf16[2048,2048]{1,0:T(8,128)(2,1)} async-done(((bf16[32,2048]{1,0:T(8,128)(2,1)}), bf16[2048,2048]{1,0:T(8,128)(2,1)}) %all-gather.2.cloned.1.call-update) | async-done | bytes 8388624 | tf_op jit(solution)/shard_map/all_gather | solution.py:13
  114.7 5.2 %fusion.36 = (bf16[2048,512]{1,0:T(8,128)(2,1)}, bf16[2048,512]{1,0:T(8,128)(2,1)}, bf16[2048,512]{1,0:T(8,128)(2,1)S(1)}, bf16[2048,512]{1,0:T(8,128)(2,1)S(1)}) fusion(bf16[2048,2048]{1,0:T(8,128)(2,1)} %all-gather.2.cloned.1.call-done), kind=kLoop, calls=%fused_computation.76 | loop fusion | bytes 16777216 | tf_op jit(solution)/shard_map/slice | solution.py:15
  120.1 1.5 copy.86
  122.0 1.1 copy-done
  123.7 3.8 %collective-permute-start = (f32[2,256]{0,1:T(8,128)S(1)}, f32[2,256]{0,1:T(8,128)}, u32[]{:S(2)}, u32[]{:S(2)}) collective-permute-start(f32[2,256]{0,1:T(8,128)S(1)} %slice.134), channel_id=1, source_target_pairs={{0,8},{8,16},{16,24},{24,32},{32,40},{40,48},{48,56},{56,64},{64,7... | collective-permute-start | bytes 6152 | tf_op jit(solution)/shard_map/ppermute | solution.py:41
  127.5 0.6 fusion.37
  128.1 1.4 copy.88
  129.5 4.0 %copy.65 = bf16[2048,512]{0,1:T(8,128)(2,1)} copy(bf16[2048,512]{1,0:T(8,128)(2,1)} %get-tuple-element.10) | data formatting | bytes 4194304 | tf_op jit(solution)/shard_map/reshape | solution.py:15
  133.5 4.1 %convolution_convert_fusion.1 = bf16[256,2048]{1,0:T(8,128)(2,1)} fusion(bf16[2,256,2048]{2,1,0:T(8,128)(2,1)} %bitcast.129, f32[2,256]{0,1:T(8,128)} %collective-permute-done, f32[256,256]{0,1:T(8,128)S(1)} %fusion.6, bf16[256,2048]{0,1:T(8,128)(2,1)S(1)} %bitcast.114, bf16[2,2048,256]{2,1,0:T(8,128)(2,1)} %bitcast.127, f32[256]{0:T(256)S(1)} %bitcast.148, ...), kind=kOutput, calls=%fused_computation.1 | convolution fusion | flops 538116096 | bytes 4590592 | tf_op jit(solution)/shard_map/dot_general | solution.py:98
  137.6 2.3 copy.90
  139.9 5.5 %all-to-all-start.1 = ((bf16[8,256,256]{2,1,0:T(8,128)(2,1)}), bf16[8,256,256]{2,1,0:T(8,128)(2,1)S(1)}, u32[]{:S(2)}, u32[]{:S(2)}) async-start(bf16[8,256,256]{2,1,0:T(8,128)(2,1)} %bitcast.125), calls=%async_computation.1 | async-start | bytes 2097152 | tf_op jit(solution)/shard_map/all_to_all | solution.py:52
  145.4 15.0 %all-to-all-done.1 = bf16[8,256,256]{2,1,0:T(8,128)(2,1)S(1)} async-done(((bf16[8,256,256]{2,1,0:T(8,128)(2,1)}), bf16[8,256,256]{2,1,0:T(8,128)(2,1)S(1)}, u32[]{:S(2)}, u32[]{:S(2)}) %all-to-all-start.1) | async-done | bytes 1048608 | tf_op jit(solution)/shard_map/all_to_all | solution.py:52
  160.7 0.6 broadcast_in_dim.9
  161.3 4.2 %all-to-all-start.2 = ((f32[8,1,512]{2,1,0:T(1,128)}), f32[8,1,512]{2,1,0:T(1,128)S(1)}, u32[]{:S(2)}, u32[]{:S(2)}) async-start(f32[8,1,512]{2,1,0:T(1,128)} %broadcast_in_dim.9), calls=%async_computation.2 | async-start | bytes 32768 | tf_op jit(solution)/shard_map/all_to_all | solution.py:29
  165.5 4.7 %all-to-all-done.2 = f32[8,1,512]{2,1,0:T(1,128)S(1)} async-done(((f32[8,1,512]{2,1,0:T(1,128)}), f32[8,1,512]{2,1,0:T(1,128)S(1)}, u32[]{:S(2)}, u32[]{:S(2)}) %all-to-all-start.2) | async-done | bytes 16416 | tf_op jit(solution)/shard_map/all_to_all | solution.py:29
  170.6 18.2 %all_to_all.32 = bf16[8,256,256]{1,2,0:T(8,128)(2,1)S(1)} all-to-all(bf16[8,256,256]{1,2,0:T(8,128)(2,1)S(1)} %broadcast_in_dim.10), channel_id=1, replica_groups=mesh['sp'=64,'tp'=8] {'tp'}, dimensions={0} | all-to-all | bytes 2097152 | tf_op jit(solution)/shard_map/all_to_all | solution.py:29
  189.8 2.6 %collective-permute-start.1 = (f32[2,256]{1,0:T(2,128)S(1)}, f32[2,256]{1,0:T(2,128)S(1)}, u32[]{:S(2)}, u32[]{:S(2)}) collective-permute-start(f32[2,256]{1,0:T(2,128)S(1)} %slice.142), channel_id=1, source_target_pairs={{0,8},{8,16},{16,24},{24,32},{32,40},{40,48},{48,56},{56,64},{64,7... | collective-permute-start | bytes 6152 | tf_op jit(solution)/shard_map/ppermute | solution.py:41
  192.4 0.7 collective-permute-done.1
  193.1 0.6 copy-done.10
  193.7 3.5 %convolution_convert_fusion = bf16[256,2048]{1,0:T(8,128)(2,1)} fusion(bf16[2,256,2048]{2,1,0:T(8,128)(2,1)} %bitcast.130, f32[2,256]{1,0:T(2,128)} %copy-done.10, f32[256,256]{1,0:T(8,128)S(1)} %fusion.1, bf16[256,2048]{0,1:T(8,128)(2,1)S(1)} %bitcast.117, bf16[2,2048,256]{2,1,0:T(8,128)(2,1)S(1)} %bitcast.128, f32[256]{0:T(256)S(1)} %bitcast.146, ...), kind=kOutput, calls=%fused_computation | convolution fusion | flops 538116096 | bytes 4461568 | tf_op jit(solution)/shard_map/dot_general | solution.py:98
  197.2 1.3 copy.89
  198.5 19.2 %all_to_all.33 = bf16[8,256,256]{2,1,0:T(8,128)(2,1)S(1)} all-to-all(bf16[8,256,256]{2,1,0:T(8,128)(2,1)S(1)} %bitcast.126), channel_id=1, replica_groups=mesh['sp'=64,'tp'=8] {'tp'}, dimensions={0} | all-to-all | bytes 2097152 | tf_op jit(solution)/shard_map/all_to_all | solution.py:52
  218.1 8.0 %all_to_all.34 = f32[8,1,512]{2,1,0:T(1,128)S(1)} all-to-all(f32[8,1,512]{2,1,0:T(1,128)S(1)} %broadcast_in_dim.11), channel_id=1, replica_groups=mesh['sp'=64,'tp'=8] {'tp'}, dimensions={0} | all-to-all | bytes 32768 | tf_op jit(solution)/shard_map/all_to_all | solution.py:29
  226.2 0.8 add_convert_fusion
  (47 shorter events, 3.2 us)
Async XLA Ops:
  6.5 108.2 %all-gather.2.cloned.1.call-start = ((), (), s32[]{:S(2)}) async-start(), calls=%async_computation.6 | async-start | bytes 8519680 | tf_op jit(solution)/shard_map/all_gather | solution.py:13
  12.4 109.2 %all-to-all-start = ((bf16[8,256,256]{1,2,0:T(8,128)(2,1)}), bf16[8,256,256]{1,2,0:T(8,128)(2,1)S(1)}, u32[]{:S(2)}, u32[]{:S(2)}) async-start(bf16[8,256,256]{1,2,0:T(8,128)(2,1)} %broadcast_in_dim.8), calls=%async_computation | async-start | bytes 2097152 | tf_op jit(solution)/shard_map/all_to_all | solution.py:29
  121.6 1.6 copy-start
  121.6 5.9 %copy-start.5 = (f32[2,3,256]{2,0,1:T(2,128)S(1)}, f32[2,3,256]{2,0,1:T(2,128)}, u32[]{:S(2)}) copy-start(f32[2,3,256]{2,0,1:T(2,128)} %param.12) | copy-start | bytes 18436
  121.6 6.5 %copy-start.2 = (bf16[2048,512]{1,0:T(8,128)(2,1)S(1)}, bf16[2048,512]{1,0:T(8,128)(2,1)}, u32[]{:S(2)}) copy-start(bf16[2048,512]{1,0:T(8,128)(2,1)} %get-tuple-element.9) | copy-start | bytes 6291460
  123.7 9.8 %collective-permute-start = (f32[2,256]{0,1:T(8,128)S(1)}, f32[2,256]{0,1:T(8,128)}, u32[]{:S(2)}, u32[]{:S(2)}) collective-permute-start(f32[2,256]{0,1:T(8,128)S(1)} %slice.134), channel_id=1, source_target_pairs={{0,8},{8,16},{16,24},{24,32},{32,40},{40,48},{48,56},{56,64},{64,7... | collective-permute-start | bytes 6152 | tf_op jit(solution)/shard_map/ppermute | solution.py:41
  137.6 7.8 %copy-start.6 = (f32[2,256]{1,0:T(2,128)S(1)}, f32[2,256]{1,0:T(2,128)}, u32[]{:S(2)}) copy-start(f32[2,256]{1,0:T(2,128)} %param.14) | copy-start | bytes 6148
  139.9 20.6 %copy-start.4 = (bf16[256,256]{1,0:T(8,128)(2,1)S(1)}, bf16[256,256]{1,0:T(8,128)(2,1)}, u32[]{:S(2)}) copy-start(bf16[256,256]{1,0:T(8,128)(2,1)} %param.8) | copy-start | bytes 393220
  139.9 25.6 %copy-start.7 = (f32[2,256]{1,0:T(2,128)S(1)}, f32[2,256]{1,0:T(2,128)}, u32[]{:S(2)}) copy-start(f32[2,256]{1,0:T(2,128)} %param.15) | copy-start | bytes 6148
  139.9 20.5 %all-to-all-start.1 = ((bf16[8,256,256]{2,1,0:T(8,128)(2,1)}), bf16[8,256,256]{2,1,0:T(8,128)(2,1)S(1)}, u32[]{:S(2)}, u32[]{:S(2)}) async-start(bf16[8,256,256]{2,1,0:T(8,128)(2,1)} %bitcast.125), calls=%async_computation.1 | async-start | bytes 2097152 | tf_op jit(solution)/shard_map/all_to_all | solution.py:52
  161.3 8.9 %all-to-all-start.2 = ((f32[8,1,512]{2,1,0:T(1,128)}), f32[8,1,512]{2,1,0:T(1,128)S(1)}, u32[]{:S(2)}, u32[]{:S(2)}) async-start(f32[8,1,512]{2,1,0:T(1,128)} %broadcast_in_dim.9), calls=%async_computation.2 | async-start | bytes 32768 | tf_op jit(solution)/shard_map/all_to_all | solution.py:29
  170.6 18.7 %copy-start.1 = (bf16[256,2,8,256]{3,2,0,1:T(8,128)(2,1)S(1)}, bf16[256,2,8,256]{3,2,0,1:T(8,128)(2,1)}, u32[]{:S(2)}) copy-start(bf16[256,2,8,256]{3,2,0,1:T(8,128)(2,1)} %copy.86) | copy-start | bytes 6291460
  188.8 4.9 %copy-start.8 = (f32[1,1,256]{2,0,1:T(1,128)S(1)}, f32[1,1,256]{2,0,1:T(1,128)}, u32[]{:S(2)}) copy-start(f32[1,1,256]{2,0,1:T(1,128)} %get-tuple-element.13) | copy-start | bytes 3076
  188.8 4.9 %copy-start.9 = (f32[1,1,256]{2,0,1:T(1,128)S(1)}, f32[1,1,256]{2,0,1:T(1,128)}, u32[]{:S(2)}) copy-start(f32[1,1,256]{2,0,1:T(1,128)} %get-tuple-element.17) | copy-start | bytes 3076
  189.2 4.4 %copy-start.3 = (bf16[256,2,8,256]{3,2,0,1:T(8,128)(2,1)S(1)}, bf16[256,2,8,256]{3,2,0,1:T(8,128)(2,1)}, u32[]{:S(2)}) copy-start(bf16[256,2,8,256]{3,2,0,1:T(8,128)(2,1)} %copy.88) | copy-start | bytes 6291460
  189.8 3.3 %collective-permute-start.1 = (f32[2,256]{1,0:T(2,128)S(1)}, f32[2,256]{1,0:T(2,128)S(1)}, u32[]{:S(2)}, u32[]{:S(2)}) collective-permute-start(f32[2,256]{1,0:T(2,128)S(1)} %slice.142), channel_id=1, source_target_pairs={{0,8},{8,16},{16,24},{24,32},{32,40},{40,48},{48,56},{56,64},{64,7... | collective-permute-start | bytes 6152 | tf_op jit(solution)/shard_map/ppermute | solution.py:41
  193.1 0.6 copy-start.10
Sparse Core Ops, SparseCore 0:
  10.4 104.3 all-gather.1
where the time goes:
time: 236 us; the launch traced here: 234 us
  waiting for transfers between devices  112 us (47%)
  blocking collectives  45.5 us (19%)
  starting transfers between devices  26.4 us (11%)
  local copies, waits for them, and re-layouts  24.2 us (10%)
  between operations  13.6 us (6%)
  matrix products  9.49 us (4%)
    all_gather x1, waiting for transfers between devices, gather_turned(): lax.all_gather(both, axis, axis=0, tiled=True)  92.1 us
    all_to_all x2, blocking collectives, sent_to_all(): lax.all_to_all(jnp.broadcast_to(array[None], (peers, *array.shape)), axis...  26.2 us
    all_to_all x1, blocking collectives, summed_on_arrival(): tiles = lax.all_to_all(in_blocks(array, dim, peers), axis, 0, 0, tiled=True)  19.2 us
    all_to_all x1, waiting for transfers between devices, summed_on_arrival(): tiles = lax.all_to_all(in_blocks(array, dim, peers), axis, 0, 0, tiled=True)  15 us
    all_to_all x2, starting transfers between devices, sent_to_all(): lax.all_to_all(jnp.broadcast_to(array[None], (peers, *array.shape)), axis...  14.5 us
    dot_general x2, matrix products, shards(): jnp.dot(gated, all_output[layer], preferred_element_type=jnp.float32)  7.61 us
    reshape x4, local copies, waits for them, and re-layouts, gather_turned(): share = whole[:, at:at + t[0].size].reshape(-1, *t.shape[1:])  7.03 us
    ppermute x2, starting transfers between devices, from_behind(): return lax.ppermute(array, axis, pairs)  6.37 us
  transfers between devices with their start and end apart: 6, of which 4 were waited for; matrix products, arithmetic and copies ran while one was open for 6% of the time, Pallas kernels for 0%

commit v1 on v0

v1 whole, which is shorter than its diff:
```python
import jax
import jax.numpy as jnp
from jax import lax
from jax.sharding import Mesh, PartitionSpec as P

D = 2048
LAYERS = 2
TP = ("x", "core")
SP = ("z", "y")
HALO = 16
IN_UP, OUT_UP = 2.0**18, 2.0**14


def bf(x):
    return x.astype(jnp.bfloat16)


def f32(x):
    return x.astype(jnp.float32)


def rounded(x):
    return lax.reduce_precision(x, exponent_bits=8, mantissa_bits=7)


def thirds(x):
    a = rounded(x)
    b = rounded(x - a)
    c = rounded(x - a - b)
    return jnp.stack([bf(a), bf(b), bf(c)])


def packed(value, outer, inner, out, layer):
    return jnp.concatenate([value[layer], outer[layer], inner[layer], out[layer].T], axis=1)


def norm(pre, gain, bias):
    mean = jnp.mean(pre, axis=-1, keepdims=True)
    cent = pre - mean
    var = jnp.mean(cent * cent, axis=-1, keepdims=True)
    return bf(cent * lax.rsqrt(var + 1e-05) * gain + bias)


def gated_rows(x, w_in, down, taps, first, head):
    width = w_in.shape[1] // 3
    acc = jnp.dot(x, w_in, preferred_element_type=jnp.float32) * down
    u, outer, inner = (f32(bf(acc[:, i * width : (i + 1) * width])) for i in range(3))
    z = inner * u
    row = lax.broadcasted_iota(jnp.int32, z.shape, 0)
    z = jnp.where(jnp.logical_and(first, row < head), 0.0, z)
    conv = taps[2] * z[2:] + taps[1] * z[1:-1] + taps[0] * z[:-2]
    return bf(outer[2:] * conv)


def out_product(g, w_out_t, down):
    return lax.dot_general(g, w_out_t, (((1,), (1,)), ((), ())), preferred_element_type=jnp.float32) * down


def pair_sum(main, extra, w_out_t, down, core):
    blocks = main.reshape(4, 2, 32, -1)
    mine = jnp.where(core == 0, blocks[:, 0], blocks[:, 1]).reshape(128, -1)
    other = jnp.where(core == 0, blocks[:, 1], blocks[:, 0]).reshape(128, -1)
    if extra is not None:
        mine = jnp.concatenate([mine, extra], axis=0)
        other = jnp.concatenate([other, extra], axis=0)
    sent = bf(out_product(other, w_out_t, down))
    got = lax.ppermute(sent, "core", [(0, 1), (1, 0)])
    return out_product(mine, w_out_t, down) + f32(got)


def shards(tokens, value, outer, inner, taps, out, gain, bias):
    alpha = (2.0 * LAYERS) ** 0.25
    core = lax.axis_index("core")
    sp = lax.axis_index(SP)
    tp = lax.axis_index(TP)
    first = sp == 0
    late = lax.all_gather(packed(value, outer, inner, out, 1), SP, axis=0, tiled=True)

    halo = lax.ppermute(tokens[-HALO:], SP, [(i, i + 1) for i in range(63)])
    params = jnp.concatenate([gain, bias], axis=0)
    parts = thirds(params).reshape(12, 256)
    parts = jnp.concatenate([parts, jnp.zeros((4, 256), jnp.bfloat16)], axis=0)
    mine = jnp.concatenate([halo, tokens, parts], axis=0)
    everyone = lax.all_to_all(jnp.broadcast_to(mine[None], (8, *mine.shape)), TP, 0, 0, tiled=True)

    scale = jnp.where(jnp.arange(1024) < 768, IN_UP, OUT_UP)
    early = (f32(packed(value, outer, inner, out, 0)) * scale).astype(jnp.float16)
    early = lax.all_gather(early, SP, axis=0, tiled=True)
    early = bf(early)

    whole = jnp.moveaxis(everyone, 0, 1).reshape(288, D)
    table = f32(whole[272:284]).reshape(3, 4, D)
    table = table[0] + table[1] + table[2]
    x0 = whole[:272]

    g = gated_rows(x0, early[:, :768], 1.0 / IN_UP, taps[0], first, HALO)
    branch = pair_sum(g[HALO - 2 :], g[HALO - 10 : HALO - 2], early[:, 768:], 1.0 / OUT_UP, core)
    main = bf(branch[:128]).reshape(4, 32, D)
    extra = bf(branch[134:136]).reshape(32, 128)
    send = jnp.concatenate([main, jnp.broadcast_to(extra[None], (4, 32, 128))], axis=2)
    got = jnp.sum(f32(lax.all_to_all(send, "x", 0, 0, tiled=True)), axis=0)
    own = lax.dynamic_slice_in_dim(x0, HALO + 32 * tp, 32, axis=0)
    pre = jnp.concatenate([alpha * f32(own) + got[:, :D], alpha * f32(x0[HALO - 2 : HALO]) + got[:, D:].reshape(2, D)], axis=0)
    state = norm(pre, table[0], table[2])
    own = state[:32]
    every = lax.all_gather(own.astype(jnp.float16), TP, axis=0, tiled=True)
    x1 = jnp.concatenate([jnp.zeros((6, D), jnp.bfloat16), state[32:], bf(every)], axis=0)

    g = gated_rows(x1, late[:, :768], 1.0, taps[1], first, 8)
    branch = pair_sum(g[6:], None, late[:, 768:], 1.0, core)
    got = lax.all_to_all(bf(branch).reshape(4, 32, D), "x", 0, 0, tiled=True)
    pre = alpha * f32(own) + jnp.sum(f32(got), axis=0)
    state = norm(pre, table[1], table[3])
    back = jnp.moveaxis(state.reshape(32, 8, 256), 1, 0)
    return lax.all_to_all(back, TP, 0, 0, tiled=True).reshape(256, 256)


def solution(mesh):
    mesh = Mesh(mesh.devices.reshape(8, 8, 4, 2), ("z", "y", "x", "core"))
    in_specs = (
        P(SP, TP),
        P(None, SP, TP),
        P(None, SP, TP),
        P(None, SP, TP),
        P(None, None, TP),
        P(None, TP, SP),
        P(None, TP),
        P(None, TP),
    )
    return jax.shard_map(shards, mesh=mesh, in_specs=in_specs, out_specs=P(SP, TP), check_vma=False)
```

time: 236 us -> 172 us (0.73)
  waiting for transfers between devices: 112 us -> 12.5 us
  blocking collectives: 45.5 us -> 92.5 us
  local copies, waits for them, and re-layouts: 24.2 us -> 7.43 us
  other arithmetic: 2.3 us -> 8.44 us
  starting transfers between devices: 26.4 us -> 30.1 us
  matrix products: 9.49 us -> 6.15 us
    all_gather x1, waiting for transfers between devices: 92.1 us -> 0.02 us  [shards(): lax.all_gather(packed(value, outer, inner, out, 1), SP, axis=0, tiled=True)]
    all_gather x0 -> x2, blocking collectives: none -> 72.1 us  [the longest x1 56.9 us: shards(): early = lax.all_gather(early, SP, axis=0, tiled=True)]
    all_to_all x3 -> x2, blocking collectives: 45.5 us -> 20.5 us  [the longest x1 11.7 us: shards(): got = lax.all_to_all(bf(branch).reshape(4, 32, D), 'x', 0, 0, tiled=True)]
    reshape x10 -> x2, local copies, waits for them, and re-layouts: 13.7 us -> 0.03 us  [the longest x1 0.01 us: shards(): got[:, D:].reshape(2, D)]
    ppermute x2 -> x3, starting transfers between devices: 6.37 us -> 17.3 us  [the longest x2 13.3 us: pair_sum(): got = lax.ppermute(sent, 'core', [(0, 1), (1, 0)])]
    all_to_all x3 -> x2, waiting for transfers between devices: 19.6 us -> 9.22 us  [the longest x1 9.22 us: shards(): got = jnp.sum(f32(lax.all_to_all(send, 'x', 0, 0, tiled=True)), axis=0)]
    all_to_all x3 -> x2, starting transfers between devices: 20 us -> 12.8 us  [the longest x1 8.04 us: shards(): lax.all_to_all(jnp.broadcast_to(mine[None], (8, *mine.shape)), TP, 0, 0,...]
    slice x6 -> x12, local copies, waits for them, and re-layouts: 5.87 us -> 1.06 us  [the longest x1 0.7 us: shards(): halo = lax.ppermute(tokens[-HALO:], SP, [(i, i + 1) for i in range(63)])]
  transfers between devices with their start and end apart: 6 -> 6, of which waited for: 4 -> 3; matrix products, arithmetic and copies ran while one was open for 6% -> 7% of each run, Pallas kernels for 0% -> 0%
where the time goes in v1:
time: 172 us; the launch traced here: 171 us
  blocking collectives  92.5 us (54%)
  starting transfers between devices  30.1 us (18%)
  between operations  13.8 us (8%)
  waiting for transfers between devices  12.5 us (7%)
  other arithmetic  8.44 us (5%)
  local copies, waits for them, and re-layouts  7.43 us (4%)
  matrix products  6.15 us (4%)
    all_gather x1, blocking collectives, shards(): early = lax.all_gather(early, SP, axis=0, tiled=True)  56.9 us
    all_gather x1, blocking collectives, shards(): every = lax.all_gather(own.astype(jnp.float16), TP, axis=0, tiled=True)  15.2 us
    ppermute x2, starting transfers between devices, pair_sum(): got = lax.ppermute(sent, 'core', [(0, 1), (1, 0)])  13.3 us
    all_to_all x1, blocking collectives, shards(): got = lax.all_to_all(bf(branch).reshape(4, 32, D), 'x', 0, 0, tiled=True)  11.7 us
    all_to_all x1, waiting for transfers between devices, shards(): got = jnp.sum(f32(lax.all_to_all(send, 'x', 0, 0, tiled=True)), axis=0)  9.22 us
    all_to_all x1, blocking collectives, shards(): return lax.all_to_all(back, TP, 0, 0, tiled=True).reshape(256, 256)  8.78 us
    all_to_all x1, starting transfers between devices, shards(): lax.all_to_all(jnp.broadcast_to(mine[None], (8, *mine.shape)), TP, 0, 0,...  8.04 us
    all_to_all x1, starting transfers between devices, shards(): got = jnp.sum(f32(lax.all_to_all(send, 'x', 0, 0, tiled=True)), axis=0)  4.74 us
  transfers between devices with their start and end apart: 6, of which 3 were waited for; matrix products, arithmetic and copies ran while one was open for 7% of the time, Pallas kernels for 0%

profile of v1, /device:TPU:1, one launch (start us, length us, event | category | flops | bytes accessed | tf_op | source)
XLA Modules:
  0.0 170.9 jit_solution(12494518444327532426)
XLA Ops:
  6.5 0.7 slice_bitcast_fusion.8
  7.3 0.7 slice_bitcast_fusion.5
  8.0 0.8 slice_bitcast_fusion.6
  8.8 0.6 pad_maximum_fusion.6
  9.4 0.7 slice.214
  10.1 4.0 %collective-permute-start = (bf16[16,256]{1,0:T(8,128)(2,1)S(1)}, bf16[16,256]{1,0:T(8,128)(2,1)S(1)}, u32[]{:S(2)}, u32[]{:S(2)}) collective-permute-start(bf16[16,256]{1,0:T(8,128)(2,1)S(1)} %slice.214), channel_id=1, source_target_pairs={{0,8},{8,16},{16,24},{24,32},{32,40},{40,48},{48,56},{56,64},{64,7... | collective-permute-start | bytes 24584 | tf_op jit(solution)/shard_map/ppermute | solution.py:79
  14.2 0.7 reduce-precision_convert_fusion.1
  15.0 1.0 maximum_maximum_fusion
  16.1 1.2 broadcast_in_dim.41
  17.2 8.0 %all-to-all-start = ((bf16[8,288,256]{2,1,0:T(8,128)(2,1)}), bf16[8,288,256]{2,1,0:T(8,128)(2,1)S(1)}, u32[]{:S(2)}, u32[]{:S(2)}) async-start(bf16[8,288,256]{2,1,0:T(8,128)(2,1)} %broadcast_in_dim.41), calls=%async_computation | async-start | bytes 2359296 | tf_op jit(solution)/shard_map/all_to_all | solution.py:84
  25.3 56.9 %all-gather.5 = f16[2048,1024]{1,0:T(8,128)(2,1)S(1)} all-gather(f16[32,1024]{1,0:T(8,128)(2,1)S(1)} %multiply_convert_fusion), channel_id=1, replica_groups=mesh['z'=8,'y'=8,'x'=4,'core'=2] {'z','y'}, dimensions={0}, use_global_device_ids=true | all-gather | bytes 4259840 | tf_op jit(solution)/shard_map/all_gather | solution.py:88
  82.2 3.2 %convert_element_type.120 = bf16[2048,1024]{1,0:T(8,128)(2,1)} convert(f16[2048,1024]{1,0:T(8,128)(2,1)S(1)} %all-gather.5) | non-fusion elementwise | flops 2097152 | bytes 8388608 | tf_op jit(solution)/shard_map/convert_element_type | solution.py:15
  85.6 2.0 %copy-done = bf16[2048,1024]{1,0:T(8,128)(2,1)S(1)} copy-done((bf16[2048,1024]{1,0:T(8,128)(2,1)S(1)}, bf16[2048,1024]{1,0:T(8,128)(2,1)}, u32[]{:S(2)}) %copy-start) | copy-done | bytes 4194328
  87.6 1.1 fusion.8
  89.0 0.5 fusion.4
  89.5 11.2 %collective-permute-start.1 = (bf16[136,2048]{1,0:T(8,128)(2,1)S(1)}, bf16[136,2048]{1,0:T(8,128)(2,1)S(1)}, u32[]{:S(2)}, u32[]{:S(2)}) collective-permute-start(bf16[136,2048]{1,0:T(8,128)(2,1)S(1)} %fusion.4), channel_id=1, source_target_pairs={{0,1},{1,0},{2,3},{3,2},{4,5},{5,4},{6,7},{7,6},{8,9},{9,8},{10,11... | collective-permute-start | bytes 1671176 | tf_op jit(solution)/shard_map/ppermute | solution.py:67
  100.8 1.5 collective-permute-done.1
  102.3 0.5 add_convert_fusion
  102.9 0.9 pad_maximum_fusion
  103.8 4.7 %all-to-all-start.1 = ((bf16[4,32,2176]{2,1,0:T(8,128)(2,1)}), bf16[4,32,2176]{2,1,0:T(8,128)(2,1)S(1)}, u32[]{:S(2)}, u32[]{:S(2)}) async-start(bf16[4,32,2176]{2,1,0:T(8,128)(2,1)} %pad_maximum_fusion), calls=%async_computation.1 | async-start | bytes 1114112 | tf_op jit(solution)/shard_map/all_to_all | solution.py:101
  108.6 9.2 %all-to-all-done.1 = bf16[4,32,2176]{2,1,0:T(8,128)(2,1)S(1)} async-done(((bf16[4,32,2176]{2,1,0:T(8,128)(2,1)}), bf16[4,32,2176]{2,1,0:T(8,128)(2,1)S(1)}, u32[]{:S(2)}, u32[]{:S(2)}) %all-to-all-start.1) | async-done | bytes 557088 | tf_op jit(solution)/shard_map/all_to_all | solution.py:101
  118.1 0.2 multiply_reduce_fusion
  118.5 15.2 %all-gather.6 = f16[256,2048]{1,0:T(8,128)(2,1)S(1)} all-gather(f16[32,2048]{1,0:T(8,128)(2,1)S(1)} %slice_convert_fusion), channel_id=1, replica_groups=mesh['z'=8,'y'=8,'x'=4,'core'=2] {'x','core'}, dimensions={0}, use_global_device_ids=true | all-gather | bytes 1179648 | tf_op jit(solution)/shard_map/all_gather | solution.py:106
  134.0 3.1 %fusion.11 = bf16[264,768]{1,0:T(8,128)(2,1)S(1)} fusion(bf16[2048,1024]{1,0:T(8,128)(2,1)} %all-gather.4.cloned.1.call-done, bf16[256,2048]{1,0:T(8,128)(2,1)S(1)} %convert_element_type.132, bf16[2,2048]{1,0:T(2,128)(2,1)S(1)} %slice.296, bf16[264]{0:T(512)(128)(2,1)S(1)} %pad.4.clone), kind=kOutput, calls=%fused_computation.10 | convolution fusion | flops 833918976 | bytes 4608528 | tf_op jit(solution)/shard_map/dot_general | solution.py:46
  137.5 0.5 convolution_convert_fusion
  138.0 2.1 %collective-permute-start.2 = (bf16[128,2048]{1,0:T(8,128)(2,1)S(1)}, bf16[128,2048]{1,0:T(8,128)(2,1)S(1)}, u32[]{:S(2)}, u32[]{:S(2)}) collective-permute-start(bf16[128,2048]{1,0:T(8,128)(2,1)S(1)} %convolution_convert_fusion), channel_id=1, source_target_pairs={{0,1},{1,0},{2,3},{3,2},{4,5},{5,4},{6,7},{7,6},{8,9},{9,8},{10,11... | collective-permute-start | bytes 1572872 | tf_op jit(solution)/shard_map/ppermute | solution.py:67
  140.1 1.7 %collective-permute-done.2 = bf16[128,2048]{1,0:T(8,128)(2,1)S(1)} collective-permute-done((bf16[128,2048]{1,0:T(8,128)(2,1)S(1)}, bf16[128,2048]{1,0:T(8,128)(2,1)S(1)}, u32[]{:S(2)}, u32[]{:S(2)}) %collective-permute-start.2) | collective-permute-done | bytes 524320 | tf_op jit(solution)/shard_map/ppermute | solution.py:67
  141.8 0.5 add_convert_fusion.1
  142.3 11.7 %all_to_all.20 = bf16[4,32,2048]{2,1,0:T(8,128)(2,1)S(1)} all-to-all(bf16[4,32,2048]{2,1,0:T(8,128)(2,1)S(1)} %bitcast.57), channel_id=1, replica_groups=mesh['z'=8,'y'=8,'x'=4,'core'=2] {'x'}, dimensions={0} | all-to-all | bytes 1048576 | tf_op jit(solution)/shard_map/all_to_all | solution.py:111
  154.2 0.2 multiply_reduce_fusion.1
  154.7 8.8 %all_to_all.21 = bf16[8,32,256]{2,1,0:T(8,128)(2,1)S(1)} all-to-all(bf16[8,32,256]{2,1,0:T(8,128)(2,1)S(1)} %copy.11), channel_id=1, replica_groups=mesh['z'=8,'y'=8,'x'=4,'core'=2] {'x','core'}, dimensions={0} | all-to-all | bytes 262144 | tf_op jit(solution)/shard_map/all_to_all | solution.py:115
  163.4 0.7 copy.15
  (60 shorter events, 2.3 us)
Async XLA Ops:
  6.5 127.5 %all-gather.4.cloned.1.call-start = ((), (), s32[]{:S(2)}) async-start(), calls=%async_computation.4 | async-start | bytes 4259840 | tf_op jit(solution)/shard_map/all_gather | solution.py:77
  10.1 4.9 %collective-permute-start = (bf16[16,256]{1,0:T(8,128)(2,1)S(1)}, bf16[16,256]{1,0:T(8,128)(2,1)S(1)}, u32[]{:S(2)}, u32[]{:S(2)}) collective-permute-start(bf16[16,256]{1,0:T(8,128)(2,1)S(1)} %slice.214), channel_id=1, source_target_pairs={{0,8},{8,16},{16,24},{24,32},{32,40},{40,48},{48,56},{56,64},{64,7... | collective-permute-start | bytes 24584 | tf_op jit(solution)/shard_map/ppermute | solution.py:79
  17.2 68.2 %all-to-all-start = ((bf16[8,288,256]{2,1,0:T(8,128)(2,1)}), bf16[8,288,256]{2,1,0:T(8,128)(2,1)S(1)}, u32[]{:S(2)}, u32[]{:S(2)}) async-start(bf16[8,288,256]{2,1,0:T(8,128)(2,1)} %broadcast_in_dim.41), calls=%async_computation | async-start | bytes 2359296 | tf_op jit(solution)/shard_map/all_to_all | solution.py:84
  82.1 3.2 %copy-start.2 = (f32[2,3,256]{2,0,1:T(2,128)S(1)}, f32[2,3,256]{2,0,1:T(2,128)}, u32[]{:S(2)}) copy-start(f32[2,3,256]{2,0,1:T(2,128)} %param.12) | copy-start | bytes 18436
  85.4 2.2 %copy-start = (bf16[2048,1024]{1,0:T(8,128)(2,1)S(1)}, bf16[2048,1024]{1,0:T(8,128)(2,1)}, u32[]{:S(2)}) copy-start(bf16[2048,1024]{1,0:T(8,128)(2,1)} %convert_element_type.120) | copy-start | bytes 12582916
  89.5 12.8 %collective-permute-start.1 = (bf16[136,2048]{1,0:T(8,128)(2,1)S(1)}, bf16[136,2048]{1,0:T(8,128)(2,1)S(1)}, u32[]{:S(2)}, u32[]{:S(2)}) collective-permute-start(bf16[136,2048]{1,0:T(8,128)(2,1)S(1)} %fusion.4), channel_id=1, source_target_pairs={{0,1},{1,0},{2,3},{3,2},{4,5},{5,4},{6,7},{7,6},{8,9},{9,8},{10,11... | collective-permute-start | bytes 1671176 | tf_op jit(solution)/shard_map/ppermute | solution.py:67
  103.8 14.0 %all-to-all-start.1 = ((bf16[4,32,2176]{2,1,0:T(8,128)(2,1)}), bf16[4,32,2176]{2,1,0:T(8,128)(2,1)S(1)}, u32[]{:S(2)}, u32[]{:S(2)}) async-start(bf16[4,32,2176]{2,1,0:T(8,128)(2,1)} %pad_maximum_fusion), calls=%async_computation.1 | async-start | bytes 1114112 | tf_op jit(solution)/shard_map/all_to_all | solution.py:101
  134.0 3.5 %copy-start.1 = (bf16[2048,1024]{1,0:T(8,128)(2,1)S(1)}, bf16[2048,1024]{1,0:T(8,128)(2,1)}, u32[]{:S(2)}) copy-start(bf16[2048,1024]{1,0:T(8,128)(2,1)} %all-gather.4.cloned.1.call-done) | copy-start | bytes 12582916
  138.0 3.8 %collective-permute-start.2 = (bf16[128,2048]{1,0:T(8,128)(2,1)S(1)}, bf16[128,2048]{1,0:T(8,128)(2,1)S(1)}, u32[]{:S(2)}, u32[]{:S(2)}) collective-permute-start(bf16[128,2048]{1,0:T(8,128)(2,1)S(1)} %convolution_convert_fusion), channel_id=1, source_target_pairs={{0,1},{1,0},{2,3},{3,2},{4,5},{5,4},{6,7},{7,6},{8,9},{9,8},{10,11... | collective-permute-start | bytes 1572872 | tf_op jit(solution)/shard_map/ppermute | solution.py:67
Sparse Core Ops, SparseCore 0:
  10.4 93.0 all-gather.3

commit v2 on v1

v2 whole, which is shorter than its diff:
```python
import jax
import jax.numpy as jnp
from jax import lax
from jax.experimental import pallas as pl
from jax.experimental.pallas import tpu as pltpu
from jax.sharding import Mesh, PartitionSpec as P


D = 2048
LAYERS = 2
TP = ("x", "core")
SP = ("z", "y")
HALO = 16
IN_UP, OUT_UP = 2.0**18, 2.0**14


def bf(x):
    return x.astype(jnp.bfloat16)


def f32(x):
    return x.astype(jnp.float32)


def fetch(sources, targets, sems):
    copies = [pltpu.make_async_copy(a, b, sems.at[i]) for i, (a, b) in enumerate(zip(sources, targets))]
    for copy in copies:
        copy.start()
    for copy in copies:
        copy.wait()


HBM = pl.BlockSpec(memory_space=pltpu.HBM)
VMEM = pl.BlockSpec(memory_space=pltpu.VMEM)


def pack_kernel(value, outer, inner, out_t, early, late, held, sems):
    fetch((value, outer, inner, out_t), [held.at[i] for i in range(4)], sems)
    for i in range(4):
        at = slice(256 * i, 256 * (i + 1))
        early[:, at] = bf(f32(held[i, 0]) * (IN_UP if i < 3 else OUT_UP))
        late[:, at] = held[i, 1]


def pack(value, outer, inner, out_t):
    shape = jax.ShapeDtypeStruct((32, 1024), jnp.bfloat16)
    return pl.pallas_call(
        pack_kernel,
        in_specs=[HBM] * 4,
        out_specs=(VMEM, VMEM),
        out_shape=(shape, shape),
        scratch_shapes=[pltpu.VMEM((4, 2, 32, 256), jnp.bfloat16), pltpu.SemaphoreType.DMA((4,))],
        cost_estimate=pl.CostEstimate(flops=2000000, bytes_accessed=262144, transcendentals=0),
    )(value, outer, inner, out_t)


def stack_kernel(halo, tokens, gain, bias, copies, held, left, sems):
    fetch((tokens, gain, bias), (held.at[HALO : HALO + 256], left.at[0:2], left.at[2:4]), sems)
    held[:HALO] = halo[...]
    rest = left[...]
    terms = []
    for _ in range(3):
        terms.append(f32(bf(rest)))
        rest = rest - terms[-1]
    terms.append(jnp.zeros_like(rest))
    held[HALO + 256 :] = bf(jnp.concatenate(terms, axis=0))
    fetch([held] * 8, [copies.at[i] for i in range(8)], sems)


def stacked_copies(halo, tokens, gain, bias):
    return pl.pallas_call(
        stack_kernel,
        in_specs=[VMEM, HBM, HBM, HBM],
        out_specs=HBM,
        out_shape=jax.ShapeDtypeStruct((8, 288, 256), jnp.bfloat16),
        scratch_shapes=[
            pltpu.VMEM((288, 256), jnp.bfloat16),
            pltpu.VMEM((4, 256), jnp.float32),
            pltpu.SemaphoreType.DMA((8,)),
        ],
        cost_estimate=pl.CostEstimate(flops=2000000, bytes_accessed=1400000, transcendentals=0),
    )(halo, tokens, gain, bias)


def norm(pre, gain, bias):
    mean = jnp.mean(pre, axis=-1, keepdims=True)
    cent = pre - mean
    var = jnp.mean(cent * cent, axis=-1, keepdims=True)
    return bf(cent * lax.rsqrt(var + 1e-05) * gain + bias)


def shards(tokens, value, outer, inner, taps, out, gain, bias):
    taps = jnp.swapaxes(taps, 0, 1)
    halo = lax.ppermute(tokens[-HALO:], SP, [(i, i + 1) for i in range(63)])
    early, late = pack(value, outer, inner, jnp.swapaxes(out, 1, 2))
    late = lax.all_gather(late, SP, axis=0, tiled=True)
    copies = stacked_copies(halo, tokens, gain, bias)
    everyone = lax.all_to_all(copies, TP, 0, 0, tiled=True)
    early = lax.all_gather(early.astype(jnp.float16), SP, axis=0, tiled=True)

    early, everyone = lax.optimization_barrier((early, everyone))
    sent, mine, kept, table = front(everyone, [bf(early[:, 256 * i : 256 * (i + 1)]) for i in range(4)], taps)
    got = lax.ppermute(sent, "core", [(0, 1), (1, 0)])
    got = lax.all_to_all(folded(got, mine), "x", 0, 0, tiled=True)
    own, before = middle(got, kept, table)
    every = lax.all_gather(own.astype(jnp.float16), TP, axis=0, tiled=True)

    sent, mine = rear(bf(every), before, late, taps)
    got = lax.ppermute(sent, "core", [(0, 1), (1, 0)])
    got = lax.all_to_all(bf(f32(got) + mine).reshape(4, 32, D), "x", 0, 0, tiled=True)
    return lax.all_to_all(last(got, own, table), TP, 0, 0, tiled=True).reshape(256, 256)


def front_kernel(xs, w_u, w_outer, w_inner, w_out, taps, sent, mine, kept, table, x, g, half):
    core = lax.axis_index("core")
    tp = 2 * lax.axis_index("x") + core
    first = jnp.logical_and(lax.axis_index("z") == 0, lax.axis_index("y") == 0)
    rows = HALO + 256
    for j in range(8):
        x[:, 256 * j : 256 * (j + 1)] = xs[j, :rows]
        tail = f32(xs[j, rows:])
        table[:, 256 * j : 256 * (j + 1)] = tail[0:4] + tail[4:8] + tail[8:12]
    u, outer, inner = (
        f32(bf(jnp.dot(x[...], w[...], preferred_element_type=jnp.float32) * (1.0 / IN_UP)))
        for w in (w_u, w_outer, w_inner)
    )
    row = lax.broadcasted_iota(jnp.int32, u.shape, 0)
    z = jnp.where(jnp.logical_and(first, row < HALO), 0.0, inner * u)
    conv = taps[2, 0:1] * z + taps[1, 0:1] * pltpu.roll(z, 1, 0) + taps[0, 0:1] * pltpu.roll(z, 2, 0)
    g[...] = bf(outer * conv)
    alpha = (2.0 * LAYERS) ** 0.25
    kept[:32] = alpha * f32(x[pl.ds(pl.multiple_of(HALO + 32 * tp, 16), 32)])
    kept[32:] = alpha * f32(x[HALO - 8 : HALO])
    half[128:] = g[HALO - 8 : HALO]
    for target, which in ((sent, 1 - core), (mine, core)):
        for i in range(4):
            half[32 * i : 32 * (i + 1)] = g[pl.ds(pl.multiple_of(HALO + 64 * i + 32 * which, 16), 32)]
        for n in range(4):
            at = slice(512 * n, 512 * (n + 1))
            part = lax.dot_general(
                half[...], w_out[at], (((1,), (1,)), ((), ())), preferred_element_type=jnp.float32
            ) * (1.0 / OUT_UP)
            target[:, at] = part.astype(target.dtype)


def front(xs, weights, taps):
    shape = jax.ShapeDtypeStruct
    return pl.pallas_call(
        front_kernel,
        out_shape=(
            shape((136, D), jnp.bfloat16),
            shape((136, D), jnp.float32),
            shape((40, D), jnp.float32),
            shape((4, D), jnp.float32),
        ),
        scratch_shapes=[
            pltpu.VMEM((HALO + 256, D), jnp.bfloat16),
            pltpu.VMEM((HALO + 256, 256), jnp.bfloat16),
            pltpu.VMEM((136, 256), jnp.bfloat16),
        ],
        compiler_params=pltpu.CompilerParams(vmem_limit_bytes=20 * 2**20),
        cost_estimate=pl.CostEstimate(flops=1200000000, bytes_accessed=7000000, transcendentals=0),
    )(xs, *weights, taps)


def fold_kernel(got, mine, out, strip):
    total = f32(got[...]) + mine[...]
    for i in range(4):
        out[i, :, :D] = bf(total[32 * i : 32 * (i + 1)])
    for t in range(2):
        for r in range(16):
            strip[16 * t + r : 16 * t + r + 1] = total[134 + t : 135 + t, 128 * r : 128 * (r + 1)]
    for i in range(4):
        out[i, :, D:] = bf(strip[...])


def folded(got, mine):
    return pl.pallas_call(
        fold_kernel,
        out_shape=jax.ShapeDtypeStruct((4, 32, D + 128), jnp.bfloat16),
        scratch_shapes=[pltpu.VMEM((32, 128), jnp.float32)],
        compiler_params=pltpu.CompilerParams(vmem_limit_bytes=6 * 2**20),
        cost_estimate=pl.CostEstimate(flops=1000000, bytes_accessed=2200000, transcendentals=0),
    )(got, mine)


def middle_kernel(got, kept, table, own, before, wide):
    total = f32(got[0]) + f32(got[1]) + f32(got[2]) + f32(got[3])
    wide[...] = jnp.zeros_like(wide)
    for t in range(2):
        for r in range(16):
            wide[6 + t : 7 + t, 128 * r : 128 * (r + 1)] = total[16 * t + r : 16 * t + r + 1, D:]
    gain, bias = table[0:1], table[2:3]
    own[...] = norm(kept[:32] + total[:, :D], gain, bias)
    before[...] = norm(kept[32:] + wide[...], gain, bias)


def middle(got, kept, table):
    shape = jax.ShapeDtypeStruct
    return pl.pallas_call(
        middle_kernel,
        out_shape=(shape((32, D), jnp.bfloat16), shape((8, D), jnp.bfloat16)),
        scratch_shapes=[pltpu.VMEM((8, D), jnp.float32)],
        compiler_params=pltpu.CompilerParams(vmem_limit_bytes=6 * 2**20),
        cost_estimate=pl.CostEstimate(flops=2000000, bytes_accessed=1200000, transcendentals=100),
    )(got, kept, table)


def rear_kernel(x, before, w, taps, sent, mine, held, acc, g, half, sems):
    core = lax.axis_index("core")
    first = jnp.logical_and(lax.axis_index("z") == 0, lax.axis_index("y") == 0)
    step = D // 4
    copies = [
        pltpu.make_async_copy(w.at[step * i : step * (i + 1)], held.at[step * i : step * (i + 1)], sems.at[i])
        for i in range(4)
    ]
    for copy in copies:
        copy.start()
    for i, copy in enumerate(copies):
        copy.wait()
        at = slice(step * i, step * (i + 1))
        for rows, source in ((slice(0, 8), before), (slice(8, 264), x)):
            part = jnp.dot(source[:, at], held[at, :768], preferred_element_type=jnp.float32)
            acc[rows] = part if i == 0 else acc[rows] + part
    u, outer, inner = (f32(bf(acc[:, 256 * i : 256 * (i + 1)])) for i in range(3))
    row = lax.broadcasted_iota(jnp.int32, u.shape, 0)
    z = jnp.where(jnp.logical_and(first, row < 8), 0.0, inner * u)
    conv = taps[2, 1:2] * z + taps[1, 1:2] * pltpu.roll(z, 1, 0) + taps[0, 1:2] * pltpu.roll(z, 2, 0)
    g[...] = bf((outer * conv)[8:])
    for target, which in ((sent, 1 - core), (mine, core)):
        for i in range(4):
            half[32 * i : 32 * (i + 1)] = g[pl.ds(pl.multiple_of(64 * i + 32 * which, 16), 32)]
        for n in range(4):
            at = slice(512 * n, 512 * (n + 1))
            part = lax.dot_general(
                half[...], held[at, 768:], (((1,), (1,)), ((), ())), preferred_element_type=jnp.float32
            )
            target[:, at] = part.astype(target.dtype)


def rear(x, before, w, taps):
    shape = jax.ShapeDtypeStruct
    return pl.pallas_call(
        rear_kernel,
        in_specs=[VMEM, VMEM, HBM, VMEM],
        out_specs=(VMEM, VMEM),
        out_shape=(shape((128, D), jnp.bfloat16), shape((128, D), jnp.float32)),
        scratch_shapes=[
            pltpu.VMEM((D, 1024), jnp.bfloat16),
            pltpu.VMEM((264, 768), jnp.float32),
            pltpu.VMEM((256, 256), jnp.bfloat16),
            pltpu.VMEM((128, 256), jnp.bfloat16),
            pltpu.SemaphoreType.DMA((4,)),
        ],
        compiler_params=pltpu.CompilerParams(vmem_limit_bytes=50 * 2**20),
        cost_estimate=pl.CostEstimate(flops=1200000000, bytes_accessed=7000000, transcendentals=0),
    )(x, before, w, taps)


def last_kernel(got, own, table, out):
    total = f32(got[0]) + f32(got[1]) + f32(got[2]) + f32(got[3])
    alpha = (2.0 * LAYERS) ** 0.25
    state = norm(alpha * f32(own[...]) + total, table[1:2], table[3:4])
    for i in range(8):
        out[i] = state[:, 256 * i : 256 * (i + 1)]


def last(got, own, table):
    return pl.pallas_call(
        last_kernel,
        out_shape=jax.ShapeDtypeStruct((8, 32, 256), jnp.bfloat16),
        compiler_params=pltpu.CompilerParams(vmem_limit_bytes=6 * 2**20),
        cost_estimate=pl.CostEstimate(flops=2000000, bytes_accessed=1200000, transcendentals=100),
    )(got, own, table)


def solution(mesh):
    mesh = Mesh(mesh.devices.reshape(8, 8, 4, 2), ("z", "y", "x", "core"))
    in_specs = (
        P(SP, TP),
        P(None, SP, TP),
        P(None, SP, TP),
        P(None, SP, TP),
        P(None, None, TP),
        P(None, TP, SP),
        P(None, TP),
        P(None, TP),
    )
    return jax.shard_map(shards, mesh=mesh, in_specs=in_specs, out_specs=P(SP, TP), check_vma=False)
```

time: 172 us -> 172 us (level)
  blocking collectives: 92.5 us -> 113 us
  Pallas kernels: 0 us -> 11.2 us
  waiting for transfers between devices: 12.5 us -> 3.33 us
  starting transfers between devices: 30.1 us -> 23.9 us
  matrix products: 6.15 us -> 0 us
  local copies, waits for them, and re-layouts: 7.43 us -> 1.95 us
  other arithmetic: 8.44 us -> 4.07 us
    all_to_all x2 -> x3, blocking collectives: 20.5 us -> 35 us  [the longest x1 14.6 us: shards(): got = lax.all_to_all(folded(got, mine), 'x', 0, 0, tiled=True)]
    pallas_call x0 -> x7, Pallas kernels: none -> 11.2 us  [the longest x1 3.82 us: rear(): pl.pallas_call(rear_kernel, in_specs=[VMEM, VMEM, HBM, VMEM], out_specs=(...]
    all_to_all x2 -> x1, waiting for transfers between devices: 9.22 us -> 0.01 us  [shards(): everyone = lax.all_to_all(copies, TP, 0, 0, tiled=True)]
    dot_general x6 -> x0, matrix products: 6.15 us -> none  [the longest x2 4.19 us: gated_rows(): acc = jnp.dot(x, w_in, preferred_element_type=jnp.float32) * down]
    all_gather x1, blocking collectives: 56.9 us -> 63 us  [shards(): early = lax.all_gather(early.astype(jnp.float16), SP, axis=0, tiled=True)]
    all_to_all x2 -> x1, starting transfers between devices: 12.8 us -> 8.06 us  [shards(): everyone = lax.all_to_all(copies, TP, 0, 0, tiled=True)]
    concatenate x3 -> x0, other arithmetic: 2.51 us -> none  [the longest x1 1.01 us: shards(): mine = jnp.concatenate([halo, tokens, parts], axis=0)]
    convert_element_type x7 -> x3, other arithmetic: 4.64 us -> 3.19 us  [bf(): return x.astype(jnp.bfloat16)]
  transfers between devices with their start and end apart: 6 -> 5, of which waited for: 3 -> 2; matrix products, arithmetic and copies ran while one was open for 7% -> 3% of each run, Pallas kernels for 0% -> 3%
where the time goes in v2:
time: 172 us; the launch traced here: 171 us
  blocking collectives  113 us (66%)
  starting transfers between devices  23.9 us (14%)
  between operations  13.5 us (8%)
  Pallas kernels  11.2 us (7%)
  other arithmetic  4.07 us (2%)
  waiting for transfers between devices  3.33 us (2%)
  local copies, waits for them, and re-layouts  1.95 us (1%)
    all_gather x1, blocking collectives, shards(): early = lax.all_gather(early.astype(jnp.float16), SP, axis=0, tiled=True)  63 us
    all_gather x1, blocking collectives, shards(): every = lax.all_gather(own.astype(jnp.float16), TP, axis=0, tiled=True)  15.2 us
    all_to_all x1, blocking collectives, shards(): got = lax.all_to_all(folded(got, mine), 'x', 0, 0, tiled=True)  14.6 us
    ppermute x2, starting transfers between devices, shards(): got = lax.ppermute(sent, 'core', [(0, 1), (1, 0)])  11.8 us
    all_to_all x1, blocking collectives, shards(): lax.all_to_all(bf(f32(got) + mine).reshape(4, 32, D), 'x', 0, 0, tiled=True)  11.7 us
    all_to_all x1, blocking collectives, shards(): lax.all_to_all(last(got, own, table), TP, 0, 0, tiled=True)  8.78 us
    all_to_all x1, starting transfers between devices, shards(): everyone = lax.all_to_all(copies, TP, 0, 0, tiled=True)  8.06 us
    ppermute x1, starting transfers between devices, shards(): halo = lax.ppermute(tokens[-HALO:], SP, [(i, i + 1) for i in range(63)])  4.01 us
  transfers between devices with their start and end apart: 5, of which 2 were waited for; matrix products, arithmetic and copies ran while one was open for 3% of the time, Pallas kernels for 3%

profile of v2, /device:TPU:1, one launch (start us, length us, event | category | flops | bytes accessed | tf_op | source)
XLA Modules:
  0.0 171.2 jit_solution(7162781551365055596)
XLA Ops:
  6.5 0.0 all-gather.4.cloned.1.call-start
  6.5 1.5 shard_map.82
  8.0 0.0 all-gather.4.cloned.1.call-update
  8.1 0.7 slice.15
  8.8 4.0 %collective-permute-start = (bf16[16,256]{1,0:T(8,128)(2,1)S(1)}, bf16[16,256]{1,0:T(8,128)(2,1)S(1)}, u32[]{:S(2)}, u32[]{:S(2)}) collective-permute-start(bf16[16,256]{1,0:T(8,128)(2,1)S(1)} %slice.15), channel_id=1, source_target_pairs={{0,8},{8,16},{16,24},{24,32},{32,40},{40,48},{48,56},{56,64},{64,7... | collective-permute-start | bytes 24584 | tf_op jit(solution)/shard_map/ppermute | solution.py:94
  12.8 0.9 convert_element_type.27
  13.6 0.0 collective-permute-done.halo
  13.7 0.0 copy-start.1
  13.7 0.6 copy-done.1
  14.3 2.8 %shard_map.83 = bf16[8,288,256]{2,1,0:T(8,128)(2,1)} custom-call(bf16[16,256]{1,0:T(8,128)(2,1)} %copy-done.1, bf16[256,256]{1,0:T(8,128)(2,1)} %tokens.1, f32[2,256]{1,0:T(2,128)} %gain.1, f32[2,256]{1,0:T(2,128)} %bias.1), custom_call_target="tpu_custom_call" | custom-call | flops 2000000 | bytes 1400000 | tf_op jit(solution)/shard_map/pallas_call | solution.py:71
  17.1 8.1 %all-to-all-start = ((bf16[8,288,256]{2,1,0:T(8,128)(2,1)}), bf16[8,288,256]{2,1,0:T(8,128)(2,1)S(1)}, u32[]{:S(2)}, u32[]{:S(2)}) async-start(bf16[8,288,256]{2,1,0:T(8,128)(2,1)} %shard_map.83), calls=%async_computation | async-start | bytes 2359296 | tf_op jit(solution)/shard_map/all_to_all | solution.py:98
  25.1 63.0 %all-gather.5 = f16[2048,1024]{1,0:T(8,128)(2,1)} all-gather(f16[32,1024]{1,0:T(8,128)(2,1)S(1)} %convert_element_type.27), channel_id=1, replica_groups=mesh['z'=8,'y'=8,'x'=4,'core'=2] {'z','y'}, dimensions={0}, use_global_device_ids=true | all-gather | bytes 4259840 | tf_op jit(solution)/shard_map/all_gather | solution.py:99
  88.1 0.0 all-to-all-done.xs
  88.1 3.0 %slice_convert_fusion = (bf16[2048,256]{1,0:T(8,128)(2,1)S(1)}, bf16[2048,256]{1,0:T(8,128)(2,1)S(1)}, bf16[2048,256]{1,0:T(8,128)(2,1)S(1)}, bf16[2048,256]{1,0:T(8,128)(2,1)S(1)}) fusion(f16[2048,1024]{1,0:T(8,128)(2,1)} %all-gather.5), kind=kLoop, calls=%fused_computation.1 | loop fusion | flops 2097152 | bytes 8388608 | tf_op jit(solution)/shard_map/convert_element_type | solution.py:18
  91.1 0.0 copy-done
  91.1 2.3 %shard_map.84 = (bf16[136,2048]{1,0:T(8,128)(2,1)S(1)}, f32[136,2048]{1,0:T(8,128)S(1)}, f32[40,2048]{1,0:T(8,128)S(1)}, f32[4,2048]{1,0:T(4,128)S(1)}) custom-call(bf16[8,288,256]{2,1,0:T(8,128)(2,1)S(1)} %all-to-all-done.xs, bf16[2048,256]{1,0:T(8,128)(2,1)S(1)} %get-tuple-element.32.w_u, bf16[2048,256]{1,0:T(8,128)(2,1)S(1)} %get-tuple-element.31.w_outer, ...), custom_call_target="tpu_custom_call" | custom-call | flops 1200000000 | bytes 7000000 | tf_op jit(solution)/shard_map/pallas_call | solution.py:148
  93.4 9.8 %collective-permute-start.1 = (bf16[136,2048]{1,0:T(8,128)(2,1)S(1)}, bf16[136,2048]{1,0:T(8,128)(2,1)S(1)}, u32[]{:S(2)}, u32[]{:S(2)}) collective-permute-start(bf16[136,2048]{1,0:T(8,128)(2,1)S(1)} %get-tuple-element.20), channel_id=1, source_target_pairs={{0,1},{1,0},{2,3},{3,2},{4,5},{5,4},{6,7},{7,6},{8,9},{9,8},{10,11... | collective-permute-start | bytes 1671176 | tf_op jit(solution)/shard_map/ppermute | solution.py:103
  103.1 1.6 collective-permute-done.1.got
  104.7 0.2 shard_map.85
  104.9 14.6 %all_to_all.20.got = bf16[4,32,2176]{2,1,0:T(8,128)(2,1)S(1)} all-to-all(bf16[4,32,2176]{2,1,0:T(8,128)(2,1)S(1)} %shard_map.85), channel_id=1, replica_groups=mesh['z'=8,'y'=8,'x'=4,'core'=2] {'x'}, dimensions={0} | all-to-all | bytes 1114112 | tf_op jit(solution)/shard_map/all_to_all | solution.py:104
  119.5 0.3 shard_map.86
  119.8 15.2 %all-gather.6 = f16[256,2048]{1,0:T(8,128)(2,1)S(1)} all-gather(f16[32,2048]{1,0:T(8,128)(2,1)S(1)} %convert_element_type.32), channel_id=1, replica_groups=mesh['z'=8,'y'=8,'x'=4,'core'=2] {'x','core'}, dimensions={0}, use_global_device_ids=true | all-gather | bytes 1179648 | tf_op jit(solution)/shard_map/all_gather | solution.py:106
  135.0 0.1 convert_element_type.33.x
  135.2 0.0 all-gather.4.cloned.1.call-done.w
  135.2 3.8 %shard_map.87 = (bf16[128,2048]{1,0:T(8,128)(2,1)S(1)}, f32[128,2048]{1,0:T(8,128)S(1)}) custom-call(bf16[256,2048]{1,0:T(8,128)(2,1)S(1)} %convert_element_type.33.x, bf16[8,2048]{1,0:T(8,128)(2,1)S(1)} %get-tuple-element.25.before, bf16[2048,1024]{1,0:T(8,128)(2,1)} %all-gather.4.cloned.1.call-done.w, f32[3,2,256]{2,1,0:T(2,128)S(1)} %bitcast.5), custom_call_target="tpu_custom_call" | custom-call | flops 1200000000 | bytes 7000000 | tf_op jit(solution)/shard_map/pallas_call | solution.py:243
  139.0 2.1 %collective-permute-start.2 = (bf16[128,2048]{1,0:T(8,128)(2,1)S(1)}, bf16[128,2048]{1,0:T(8,128)(2,1)S(1)}, u32[]{:S(2)}, u32[]{:S(2)}) collective-permute-start(bf16[128,2048]{1,0:T(8,128)(2,1)S(1)} %get-tuple-element.27), channel_id=1, source_target_pairs={{0,1},{1,0},{2,3},{3,2},{4,5},{5,4},{6,7},{7,6},{8,9},{9,8},{10,11... | collective-permute-start | bytes 1572872 | tf_op jit(solution)/shard_map/ppermute | solution.py:109
  141.1 1.7 %collective-permute-done.2 = bf16[128,2048]{1,0:T(8,128)(2,1)S(1)} collective-permute-done((bf16[128,2048]{1,0:T(8,128)(2,1)S(1)}, bf16[128,2048]{1,0:T(8,128)(2,1)S(1)}, u32[]{:S(2)}, u32[]{:S(2)}) %collective-permute-start.2) | collective-permute-done | bytes 524320 | tf_op jit(solution)/shard_map/ppermute | solution.py:109
  142.8 0.1 add_convert_fusion
  142.9 11.7 %all_to_all.21.got = bf16[4,32,2048]{2,1,0:T(8,128)(2,1)S(1)} all-to-all(bf16[4,32,2048]{2,1,0:T(8,128)(2,1)S(1)} %bitcast.6), channel_id=1, replica_groups=mesh['z'=8,'y'=8,'x'=4,'core'=2] {'x'}, dimensions={0} | all-to-all | bytes 1048576 | tf_op jit(solution)/shard_map/all_to_all | solution.py:110
  154.6 0.3 shard_map.88
  154.9 8.8 %all_to_all.22 = bf16[8,32,256]{2,1,0:T(8,128)(2,1)S(1)} all-to-all(bf16[8,32,256]{2,1,0:T(8,128)(2,1)S(1)} %shard_map.88), channel_id=1, replica_groups=mesh['z'=8,'y'=8,'x'=4,'core'=2] {'x','core'}, dimensions={0} | all-to-all | bytes 262144 | tf_op jit(solution)/shard_map/all_to_all | solution.py:111
  163.7 0.7 copy.10
  (2 shorter events, 0.0 us)
Async XLA Ops:
  6.5 128.7 %all-gather.4.cloned.1.call-start = ((), (), s32[]{:S(2)}) async-start(), calls=%async_computation.4 | async-start | bytes 4259840 | tf_op jit(solution)/shard_map/all_gather | solution.py:96
  8.8 4.9 %collective-permute-start = (bf16[16,256]{1,0:T(8,128)(2,1)S(1)}, bf16[16,256]{1,0:T(8,128)(2,1)S(1)}, u32[]{:S(2)}, u32[]{:S(2)}) collective-permute-start(bf16[16,256]{1,0:T(8,128)(2,1)S(1)} %slice.15), channel_id=1, source_target_pairs={{0,8},{8,16},{16,24},{24,32},{32,40},{40,48},{48,56},{56,64},{64,7... | collective-permute-start | bytes 24584 | tf_op jit(solution)/shard_map/ppermute | solution.py:94
  13.7 0.6 copy-start.1
  17.1 71.1 %all-to-all-start = ((bf16[8,288,256]{2,1,0:T(8,128)(2,1)}), bf16[8,288,256]{2,1,0:T(8,128)(2,1)S(1)}, u32[]{:S(2)}, u32[]{:S(2)}) async-start(bf16[8,288,256]{2,1,0:T(8,128)(2,1)} %shard_map.83), calls=%async_computation | async-start | bytes 2359296 | tf_op jit(solution)/shard_map/all_to_all | solution.py:98
  88.1 3.0 %copy-start = (f32[2,3,256]{2,0,1:T(2,128)S(1)}, f32[2,3,256]{2,0,1:T(2,128)}, u32[]{:S(2)}) copy-start(f32[2,3,256]{2,0,1:T(2,128)} %param.12) | copy-start | bytes 18436
  93.4 11.3 %collective-permute-start.1 = (bf16[136,2048]{1,0:T(8,128)(2,1)S(1)}, bf16[136,2048]{1,0:T(8,128)(2,1)S(1)}, u32[]{:S(2)}, u32[]{:S(2)}) collective-permute-start(bf16[136,2048]{1,0:T(8,128)(2,1)S(1)} %get-tuple-element.20), channel_id=1, source_target_pairs={{0,1},{1,0},{2,3},{3,2},{4,5},{5,4},{6,7},{7,6},{8,9},{9,8},{10,11... | collective-permute-start | bytes 1671176 | tf_op jit(solution)/shard_map/ppermute | solution.py:103
  139.0 3.8 %collective-permute-start.2 = (bf16[128,2048]{1,0:T(8,128)(2,1)S(1)}, bf16[128,2048]{1,0:T(8,128)(2,1)S(1)}, u32[]{:S(2)}, u32[]{:S(2)}) collective-permute-start(bf16[128,2048]{1,0:T(8,128)(2,1)S(1)} %get-tuple-element.27), channel_id=1, source_target_pairs={{0,1},{1,0},{2,3},{3,2},{4,5},{5,4},{6,7},{7,6},{8,9},{9,8},{10,11... | collective-permute-start | bytes 1572872 | tf_op jit(solution)/shard_map/ppermute | solution.py:109
Sparse Core Ops, SparseCore 0:
  10.4 95.1 all-gather.3

commit v3 on v2

--- a/solution.py
+++ b/solution.py
@@ -98,7 +98,6 @@
     everyone = lax.all_to_all(copies, TP, 0, 0, tiled=True)
     early = lax.all_gather(early.astype(jnp.float16), SP, axis=0, tiled=True)
 
-    early, everyone = lax.optimization_barrier((early, everyone))
     sent, mine, kept, table = front(everyone, [bf(early[:, 256 * i : 256 * (i + 1)]) for i in range(4)], taps)
     got = lax.ppermute(sent, "core", [(0, 1), (1, 0)])
     got = lax.all_to_all(folded(got, mine), "x", 0, 0, tiled=True)
@@ -107,38 +106,48 @@
 
     sent, mine = rear(bf(every), before, late, taps)
     got = lax.ppermute(sent, "core", [(0, 1), (1, 0)])
-    got = lax.all_to_all(bf(f32(got) + mine).reshape(4, 32, D), "x", 0, 0, tiled=True)
+    got = lax.all_to_all(bf(f32(got) + f32(mine)).reshape(4, 32, D), "x", 0, 0, tiled=True)
     return lax.all_to_all(last(got, own, table), TP, 0, 0, tiled=True).reshape(256, 256)
 
 
-def front_kernel(xs, w_u, w_outer, w_inner, w_out, taps, sent, mine, kept, table, x, g, half):
+def front_kernel(xs, w_u, w_outer, w_inner, w_out, taps, sent, mine, kept, table, x, tails, g, half, held, sems):
     core = lax.axis_index("core")
     tp = 2 * lax.axis_index("x") + core
     first = jnp.logical_and(lax.axis_index("z") == 0, lax.axis_index("y") == 0)
     rows = HALO + 256
+    copies = [pltpu.make_async_copy(w, held.at[i], sems.at[i]) for i, w in enumerate((w_u, w_outer, w_inner, w_out))]
     for j in range(8):
-        x[:, 256 * j : 256 * (j + 1)] = xs[j, :rows]
-        tail = f32(xs[j, rows:])
-        table[:, 256 * j : 256 * (j + 1)] = tail[0:4] + tail[4:8] + tail[8:12]
-    u, outer, inner = (
-        f32(bf(jnp.dot(x[...], w[...], preferred_element_type=jnp.float32) * (1.0 / IN_UP)))
-        for w in (w_u, w_outer, w_inner)
-    )
+        at = slice(256 * j, 256 * (j + 1))
+        copies.append(pltpu.make_async_copy(xs.at[j, 0:rows], x.at[:, at], sems.at[4 + j]))
+        copies.append(pltpu.make_async_copy(xs.at[j, rows : rows + 16], tails.at[:, at], sems.at[12 + j]))
+    for copy in copies[4:] + copies[:4]:
+        copy.start()
+    for copy in copies[4:]:
+        copy.wait()
+    tail = f32(tails[...])
+    table[...] = tail[0:4] + tail[4:8] + tail[8:12]
+    alpha = (2.0 * LAYERS) ** 0.25
+    kept[:32] = alpha * f32(x[pl.ds(pl.multiple_of(HALO + 32 * tp, 16), 32)])
+    kept[32:] = alpha * f32(x[HALO - 8 : HALO])
+    products = []
+    for i in range(3):
+        copies[i].wait()
+        part = jnp.dot(x[...], held[i], preferred_element_type=jnp.float32)
+        products.append(f32(bf(part * (1.0 / IN_UP))))
+    u, outer, inner = products
     row = lax.broadcasted_iota(jnp.int32, u.shape, 0)
     z = jnp.where(jnp.logical_and(first, row < HALO), 0.0, inner * u)
     conv = taps[2, 0:1] * z + taps[1, 0:1] * pltpu.roll(z, 1, 0) + taps[0, 0:1] * pltpu.roll(z, 2, 0)
     g[...] = bf(outer * conv)
-    alpha = (2.0 * LAYERS) ** 0.25
-    kept[:32] = alpha * f32(x[pl.ds(pl.multiple_of(HALO + 32 * tp, 16), 32)])
-    kept[32:] = alpha * f32(x[HALO - 8 : HALO])
     half[128:] = g[HALO - 8 : HALO]
+    copies[3].wait()
     for target, which in ((sent, 1 - core), (mine, core)):
         for i in range(4):
             half[32 * i : 32 * (i + 1)] = g[pl.ds(pl.multiple_of(HALO + 64 * i + 32 * which, 16), 32)]
         for n in range(4):
             at = slice(512 * n, 512 * (n + 1))
             part = lax.dot_general(
-                half[...], w_out[at], (((1,), (1,)), ((), ())), preferred_element_type=jnp.float32
+                half[...], held[3, at], (((1,), (1,)), ((), ())), preferred_element_type=jnp.float32
             ) * (1.0 / OUT_UP)
             target[:, at] = part.astype(target.dtype)
 
@@ -147,24 +156,29 @@
     shape = jax.ShapeDtypeStruct
     return pl.pallas_call(
         front_kernel,
+        in_specs=[HBM, HBM, HBM, HBM, HBM, VMEM],
+        out_specs=(VMEM,) * 4,
         out_shape=(
             shape((136, D), jnp.bfloat16),
-            shape((136, D), jnp.float32),
+            shape((136, D), jnp.bfloat16),
             shape((40, D), jnp.float32),
             shape((4, D), jnp.float32),
         ),
         scratch_shapes=[
             pltpu.VMEM((HALO + 256, D), jnp.bfloat16),
+            pltpu.VMEM((16, D), jnp.bfloat16),
             pltpu.VMEM((HALO + 256, 256), jnp.bfloat16),
             pltpu.VMEM((136, 256), jnp.bfloat16),
+            pltpu.VMEM((4, D, 256), jnp.bfloat16),
+            pltpu.SemaphoreType.DMA((20,)),
         ],
-        compiler_params=pltpu.CompilerParams(vmem_limit_bytes=20 * 2**20),
+        compiler_params=pltpu.CompilerParams(vmem_limit_bytes=49 * 2**20),
         cost_estimate=pl.CostEstimate(flops=1200000000, bytes_accessed=7000000, transcendentals=0),
     )(xs, *weights, taps)
 
 
 def fold_kernel(got, mine, out, strip):
-    total = f32(got[...]) + mine[...]
+    total = f32(got[...]) + f32(mine[...])
     for i in range(4):
         out[i, :, :D] = bf(total[32 * i : 32 * (i + 1)])
     for t in range(2):
@@ -244,7 +258,7 @@
         rear_kernel,
         in_specs=[VMEM, VMEM, HBM, VMEM],
         out_specs=(VMEM, VMEM),
-        out_shape=(shape((128, D), jnp.bfloat16), shape((128, D), jnp.float32)),
+        out_shape=(shape((128, D), jnp.bfloat16),) * 2,
         scratch_shapes=[
             pltpu.VMEM((D, 1024), jnp.bfloat16),
             pltpu.VMEM((264, 768), jnp.float32),

time: 172 us -> 168 us (0.977)
  blocking collectives: 113 us -> 108 us
  Pallas kernels: 11.2 us -> 13.8 us
    all_gather x1, blocking collectives: 63 us -> 58.4 us  [shards(): early = lax.all_gather(early.astype(jnp.float16), SP, axis=0, tiled=True)]
    pallas_call x1, Pallas kernels: 2.27 us -> 4.88 us  [front(): pl.pallas_call(front_kernel, in_specs=[HBM, HBM, HBM, HBM, HBM, VMEM], ou...]
  transfers between devices with their start and end apart: 5 -> 5, of which waited for: 2 -> 2; matrix products, arithmetic and copies ran while one was open for 3% -> 2% of each run, Pallas kernels for 3% -> 5%
where the time goes in v3:
time: 168 us; the launch traced here: 167 us
  blocking collectives  108 us (64%)
  starting transfers between devices  23.7 us (14%)
  Pallas kernels  13.8 us (8%)
  between operations  13.5 us (8%)
  waiting for transfers between devices  3.33 us (2%)
  other arithmetic  2.78 us (2%)
  local copies, waits for them, and re-layouts  1.95 us (1%)
    all_gather x1, blocking collectives, shards(): early = lax.all_gather(early.astype(jnp.float16), SP, axis=0, tiled=True)  58.4 us
    all_gather x1, blocking collectives, shards(): every = lax.all_gather(own.astype(jnp.float16), TP, axis=0, tiled=True)  15.2 us
    all_to_all x1, blocking collectives, shards(): got = lax.all_to_all(folded(got, mine), 'x', 0, 0, tiled=True)  13.9 us
    all_to_all x1, blocking collectives, shards(): lax.all_to_all(bf(f32(got) + f32(mine)).reshape(4, 32, D), 'x', 0, 0, til...  11.7 us
    ppermute x2, starting transfers between devices, shards(): got = lax.ppermute(sent, 'core', [(0, 1), (1, 0)])  11 us
    all_to_all x1, blocking collectives, shards(): lax.all_to_all(last(got, own, table), TP, 0, 0, tiled=True)  8.78 us
    all_to_all x1, starting transfers between devices, shards(): everyone = lax.all_to_all(copies, TP, 0, 0, tiled=True)  8.73 us
    pallas_call x1, Pallas kernels, front(): pl.pallas_call(front_kernel, in_specs=[HBM, HBM, HBM, HBM, HBM, VMEM], ou...  4.88 us
  transfers between devices with their start and end apart: 5, of which 2 were waited for; matrix products, arithmetic and copies ran while one was open for 2% of the time, Pallas kernels for 5%

profile of v3, /device:TPU:1, one launch (start us, length us, event | category | flops | bytes accessed | tf_op | source)
XLA Modules:
  0.0 167.0 jit_solution(5843612632527231001)
XLA Ops:
  6.5 0.0 all-gather.4.cloned.1.call-start
  6.5 1.5 shard_map.83
  8.0 0.0 all-gather.4.cloned.1.call-update
  8.1 0.7 slice.15
  8.8 4.0 %collective-permute-start = (bf16[16,256]{1,0:T(8,128)(2,1)S(1)}, bf16[16,256]{1,0:T(8,128)(2,1)S(1)}, u32[]{:S(2)}, u32[]{:S(2)}) collective-permute-start(bf16[16,256]{1,0:T(8,128)(2,1)S(1)} %slice.15), channel_id=1, source_target_pairs={{0,8},{8,16},{16,24},{24,32},{32,40},{40,48},{48,56},{56,64},{64,7... | collective-permute-start | bytes 24584 | tf_op jit(solution)/shard_map/ppermute | solution.py:94
  12.8 0.9 convert_element_type.30
  13.6 0.0 collective-permute-done.halo
  13.7 0.0 copy-start.1
  13.7 0.6 copy-done.1
  14.3 2.7 %shard_map.82 = bf16[8,288,256]{2,1,0:T(8,128)(2,1)} custom-call(bf16[16,256]{1,0:T(8,128)(2,1)} %copy-done.1, bf16[256,256]{1,0:T(8,128)(2,1)} %tokens.1, f32[2,256]{1,0:T(2,128)} %gain.1, f32[2,256]{1,0:T(2,128)} %bias.1), custom_call_target="tpu_custom_call" | custom-call | flops 2000000 | bytes 1400000 | tf_op jit(solution)/shard_map/pallas_call | solution.py:71
  17.0 8.7 %all-to-all-start = ((bf16[8,288,256]{2,1,0:T(8,128)(2,1)}), bf16[8,288,256]{2,1,0:T(8,128)(2,1)}, u32[]{:S(2)}, u32[]{:S(2)}) async-start(bf16[8,288,256]{2,1,0:T(8,128)(2,1)} %shard_map.82), calls=%async_computation | async-start | bytes 2359296 | tf_op jit(solution)/shard_map/all_to_all | solution.py:98
  25.7 58.4 %all-gather.5 = f16[2048,1024]{1,0:T(8,128)(2,1)S(1)} all-gather(f16[32,1024]{1,0:T(8,128)(2,1)S(1)} %convert_element_type.30), channel_id=1, replica_groups=mesh['z'=8,'y'=8,'x'=4,'core'=2] {'z','y'}, dimensions={0}, use_global_device_ids=true | all-gather | bytes 4259840 | tf_op jit(solution)/shard_map/all_gather | solution.py:99
  84.1 1.6 slice_convert_fusion
  85.7 0.0 all-to-all-done.xs
  85.7 0.0 copy-done
  85.7 4.9 %shard_map.84 = (bf16[136,2048]{1,0:T(8,128)(2,1)S(1)}, bf16[136,2048]{1,0:T(8,128)(2,1)S(1)}, f32[40,2048]{1,0:T(8,128)S(1)}, f32[4,2048]{1,0:T(4,128)S(1)}) custom-call(bf16[8,288,256]{2,1,0:T(8,128)(2,1)} %all-to-all-done.xs, bf16[2048,256]{1,0:T(8,128)(2,1)S(1)} %get-tuple-element.28.w_u, bf16[2048,256]{1,0:T(8,128)(2,1)S(1)} %get-tuple-element.27.w_outer, ...), custom_call_target="tpu_custom_call" | custom-call | flops 1200000000 | bytes 7000000 | tf_op jit(solution)/shard_map/pallas_call | solution.py:157
  90.6 8.9 %collective-permute-start.1 = (bf16[136,2048]{1,0:T(8,128)(2,1)S(1)}, bf16[136,2048]{1,0:T(8,128)(2,1)S(1)}, u32[]{:S(2)}, u32[]{:S(2)}) collective-permute-start(bf16[136,2048]{1,0:T(8,128)(2,1)S(1)} %get-tuple-element.16), channel_id=1, source_target_pairs={{0,1},{1,0},{2,3},{3,2},{4,5},{5,4},{6,7},{7,6},{8,9},{9,8},{10,11... | collective-permute-start | bytes 1671176 | tf_op jit(solution)/shard_map/ppermute | solution.py:102
  99.5 1.6 collective-permute-done.1.got
  101.1 0.3 shard_map.85
  101.4 13.9 %all_to_all.20.got = bf16[4,32,2176]{2,1,0:T(8,128)(2,1)S(1)} all-to-all(bf16[4,32,2176]{2,1,0:T(8,128)(2,1)S(1)} %shard_map.85), channel_id=1, replica_groups=mesh['z'=8,'y'=8,'x'=4,'core'=2] {'x'}, dimensions={0} | all-to-all | bytes 1114112 | tf_op jit(solution)/shard_map/all_to_all | solution.py:103
  115.3 0.3 shard_map.86
  115.6 15.2 %all-gather.6 = f16[256,2048]{1,0:T(8,128)(2,1)S(1)} all-gather(f16[32,2048]{1,0:T(8,128)(2,1)S(1)} %convert_element_type.35), channel_id=1, replica_groups=mesh['z'=8,'y'=8,'x'=4,'core'=2] {'x','core'}, dimensions={0}, use_global_device_ids=true | all-gather | bytes 1179648 | tf_op jit(solution)/shard_map/all_gather | solution.py:105
  130.8 0.1 convert_element_type.36.x
  131.0 0.0 all-gather.4.cloned.1.call-done.w
  131.0 3.8 %shard_map.87 = (bf16[128,2048]{1,0:T(8,128)(2,1)S(1)}, bf16[128,2048]{1,0:T(8,128)(2,1)S(1)}) custom-call(bf16[256,2048]{1,0:T(8,128)(2,1)S(1)} %convert_element_type.36.x, bf16[8,2048]{1,0:T(8,128)(2,1)S(1)} %get-tuple-element.21.before, bf16[2048,1024]{1,0:T(8,128)(2,1)} %all-gather.4.cloned.1.call-done.w, f32[3,2,256]{2,1,0:T(2,128)S(1)} %bitcast.5), custom_call_target="tpu_custom_call" | custom-call | flops 1200000000 | bytes 7000000 | tf_op jit(solution)/shard_map/pallas_call | solution.py:257
  134.8 2.1 %collective-permute-start.2 = (bf16[128,2048]{1,0:T(8,128)(2,1)S(1)}, bf16[128,2048]{1,0:T(8,128)(2,1)S(1)}, u32[]{:S(2)}, u32[]{:S(2)}) collective-permute-start(bf16[128,2048]{1,0:T(8,128)(2,1)S(1)} %get-tuple-element.23), channel_id=1, source_target_pairs={{0,1},{1,0},{2,3},{3,2},{4,5},{5,4},{6,7},{7,6},{8,9},{9,8},{10,11... | collective-permute-start | bytes 1572872 | tf_op jit(solution)/shard_map/ppermute | solution.py:108
  136.9 1.7 %collective-permute-done.2 = bf16[128,2048]{1,0:T(8,128)(2,1)S(1)} collective-permute-done((bf16[128,2048]{1,0:T(8,128)(2,1)S(1)}, bf16[128,2048]{1,0:T(8,128)(2,1)S(1)}, u32[]{:S(2)}, u32[]{:S(2)}) %collective-permute-start.2) | collective-permute-done | bytes 524320 | tf_op jit(solution)/shard_map/ppermute | solution.py:108
  138.6 0.1 add_convert_fusion
  138.8 11.7 %all_to_all.21.got = bf16[4,32,2048]{2,1,0:T(8,128)(2,1)S(1)} all-to-all(bf16[4,32,2048]{2,1,0:T(8,128)(2,1)S(1)} %bitcast.6), channel_id=1, replica_groups=mesh['z'=8,'y'=8,'x'=4,'core'=2] {'x'}, dimensions={0} | all-to-all | bytes 1048576 | tf_op jit(solution)/shard_map/all_to_all | solution.py:109
  150.4 0.3 shard_map.88
  150.8 8.8 %all_to_all.22 = bf16[8,32,256]{2,1,0:T(8,128)(2,1)S(1)} all-to-all(bf16[8,32,256]{2,1,0:T(8,128)(2,1)S(1)} %shard_map.88), channel_id=1, replica_groups=mesh['z'=8,'y'=8,'x'=4,'core'=2] {'x','core'}, dimensions={0} | all-to-all | bytes 262144 | tf_op jit(solution)/shard_map/all_to_all | solution.py:110
  159.5 0.7 copy.10
  (2 shorter events, 0.0 us)
Async XLA Ops:
  6.5 124.5 %all-gather.4.cloned.1.call-start = ((), (), s32[]{:S(2)}) async-start(), calls=%async_computation.4 | async-start | bytes 4259840 | tf_op jit(solution)/shard_map/all_gather | solution.py:96
  8.8 4.9 %collective-permute-start = (bf16[16,256]{1,0:T(8,128)(2,1)S(1)}, bf16[16,256]{1,0:T(8,128)(2,1)S(1)}, u32[]{:S(2)}, u32[]{:S(2)}) collective-permute-start(bf16[16,256]{1,0:T(8,128)(2,1)S(1)} %slice.15), channel_id=1, source_target_pairs={{0,8},{8,16},{16,24},{24,32},{32,40},{40,48},{48,56},{56,64},{64,7... | collective-permute-start | bytes 24584 | tf_op jit(solution)/shard_map/ppermute | solution.py:94
  13.7 0.6 copy-start.1
  17.0 68.7 %all-to-all-start = ((bf16[8,288,256]{2,1,0:T(8,128)(2,1)}), bf16[8,288,256]{2,1,0:T(8,128)(2,1)}, u32[]{:S(2)}, u32[]{:S(2)}) async-start(bf16[8,288,256]{2,1,0:T(8,128)(2,1)} %shard_map.82), calls=%async_computation | async-start | bytes 2359296 | tf_op jit(solution)/shard_map/all_to_all | solution.py:98
  84.1 1.6 copy-start
  90.6 10.5 %collective-permute-start.1 = (bf16[136,2048]{1,0:T(8,128)(2,1)S(1)}, bf16[136,2048]{1,0:T(8,128)(2,1)S(1)}, u32[]{:S(2)}, u32[]{:S(2)}) collective-permute-start(bf16[136,2048]{1,0:T(8,128)(2,1)S(1)} %get-tuple-element.16), channel_id=1, source_target_pairs={{0,1},{1,0},{2,3},{3,2},{4,5},{5,4},{6,7},{7,6},{8,9},{9,8},{10,11... | collective-permute-start | bytes 1671176 | tf_op jit(solution)/shard_map/ppermute | solution.py:102
  134.8 3.8 %collective-permute-start.2 = (bf16[128,2048]{1,0:T(8,128)(2,1)S(1)}, bf16[128,2048]{1,0:T(8,128)(2,1)S(1)}, u32[]{:S(2)}, u32[]{:S(2)}) collective-permute-start(bf16[128,2048]{1,0:T(8,128)(2,1)S(1)} %get-tuple-element.23), channel_id=1, source_target_pairs={{0,1},{1,0},{2,3},{3,2},{4,5},{5,4},{6,7},{7,6},{8,9},{9,8},{10,11... | collective-permute-start | bytes 1572872 | tf_op jit(solution)/shard_map/ppermute | solution.py:108
Sparse Core Ops, SparseCore 0:
  10.4 93.1 all-gather.3

commit v4 on v3

--- a/solution.py
+++ b/solution.py
@@ -22,64 +22,58 @@
     return x.astype(jnp.float32)
 
 
-def fetch(sources, targets, sems):
-    copies = [pltpu.make_async_copy(a, b, sems.at[i]) for i, (a, b) in enumerate(zip(sources, targets))]
-    for copy in copies:
-        copy.start()
-    for copy in copies:
-        copy.wait()
-
-
 HBM = pl.BlockSpec(memory_space=pltpu.HBM)
 VMEM = pl.BlockSpec(memory_space=pltpu.VMEM)
 
 
-def pack_kernel(value, outer, inner, out_t, early, late, held, sems):
-    fetch((value, outer, inner, out_t), [held.at[i] for i in range(4)], sems)
-    for i in range(4):
-        at = slice(256 * i, 256 * (i + 1))
-        early[:, at] = bf(f32(held[i, 0]) * (IN_UP if i < 3 else OUT_UP))
-        late[:, at] = held[i, 1]
-
-
-def pack(value, outer, inner, out_t):
-    shape = jax.ShapeDtypeStruct((32, 1024), jnp.bfloat16)
-    return pl.pallas_call(
-        pack_kernel,
-        in_specs=[HBM] * 4,
-        out_specs=(VMEM, VMEM),
-        out_shape=(shape, shape),
-        scratch_shapes=[pltpu.VMEM((4, 2, 32, 256), jnp.bfloat16), pltpu.SemaphoreType.DMA((4,))],
-        cost_estimate=pl.CostEstimate(flops=2000000, bytes_accessed=262144, transcendentals=0),
-    )(value, outer, inner, out_t)
-
-
-def stack_kernel(halo, tokens, gain, bias, copies, held, left, sems):
-    fetch((tokens, gain, bias), (held.at[HALO : HALO + 256], left.at[0:2], left.at[2:4]), sems)
-    held[:HALO] = halo[...]
+def pack_kernel(value, outer, inner, out_t, tokens, gain, bias, early, late, copies, held, rows, left, sems):
+    fills = [pltpu.make_async_copy(w, held.at[i], sems.at[i]) for i, w in enumerate((value, outer, inner, out_t))]
+    fills.append(pltpu.make_async_copy(gain, left.at[0:2], sems.at[4]))
+    fills.append(pltpu.make_async_copy(bias, left.at[2:4], sems.at[5]))
+    fills.append(pltpu.make_async_copy(tokens, rows.at[0:256], sems.at[6]))
+    for copy in fills[4:] + fills[:4]:
+        copy.start()
+    fills[4].wait()
+    fills[5].wait()
     rest = left[...]
     terms = []
     for _ in range(3):
         terms.append(f32(bf(rest)))
         rest = rest - terms[-1]
     terms.append(jnp.zeros_like(rest))
-    held[HALO + 256 :] = bf(jnp.concatenate(terms, axis=0))
-    fetch([held] * 8, [copies.at[i] for i in range(8)], sems)
-
-
-def stacked_copies(halo, tokens, gain, bias):
-    return pl.pallas_call(
-        stack_kernel,
-        in_specs=[VMEM, HBM, HBM, HBM],
-        out_specs=HBM,
-        out_shape=jax.ShapeDtypeStruct((8, 288, 256), jnp.bfloat16),
+    rows[256:] = bf(jnp.concatenate(terms, axis=0))
+    fills[6].wait()
+    sends = [pltpu.make_async_copy(rows, copies.at[i, HALO : HALO + 272], sems.at[7 + i]) for i in range(8)]
+    for copy in sends:
+        copy.start()
+    for i in range(4):
+        at = slice(256 * i, 256 * (i + 1))
+        fills[i].wait()
+        early[:, at] = bf(f32(held[i, 0]) * (IN_UP if i < 3 else OUT_UP))
+        late[:, at] = held[i, 1]
+    for copy in sends:
+        copy.wait()
+
+
+HBM = pl.BlockSpec(memory_space=pltpu.HBM)
+VMEM = pl.BlockSpec(memory_space=pltpu.VMEM)
+
+
+def pack(value, outer, inner, out_t, tokens, gain, bias):
+    shape = jax.ShapeDtypeStruct((32, 1024), jnp.bfloat16)
+    return pl.pallas_call(
+        pack_kernel,
+        in_specs=[HBM] * 7,
+        out_specs=(VMEM, VMEM, HBM),
+        out_shape=(shape, shape, jax.ShapeDtypeStruct((8, 288, 256), jnp.bfloat16)),
         scratch_shapes=[
-            pltpu.VMEM((288, 256), jnp.bfloat16),
+            pltpu.VMEM((4, 2, 32, 256), jnp.bfloat16),
+            pltpu.VMEM((272, 256), jnp.bfloat16),
             pltpu.VMEM((4, 256), jnp.float32),
-            pltpu.SemaphoreType.DMA((8,)),
+            pltpu.SemaphoreType.DMA((15,)),
         ],
-        cost_estimate=pl.CostEstimate(flops=2000000, bytes_accessed=1400000, transcendentals=0),
-    )(halo, tokens, gain, bias)
+        cost_estimate=pl.CostEstimate(flops=2000000, bytes_accessed=1700000, transcendentals=0),
+    )(value, outer, inner, out_t, tokens, gain, bias)
 
 
 def norm(pre, gain, bias):
@@ -92,9 +86,9 @@
 def shards(tokens, value, outer, inner, taps, out, gain, bias):
     taps = jnp.swapaxes(taps, 0, 1)
     halo = lax.ppermute(tokens[-HALO:], SP, [(i, i + 1) for i in range(63)])
-    early, late = pack(value, outer, inner, jnp.swapaxes(out, 1, 2))
+    early, late, copies = pack(value, outer, inner, jnp.swapaxes(out, 1, 2), tokens, gain, bias)
     late = lax.all_gather(late, SP, axis=0, tiled=True)
-    copies = stacked_copies(halo, tokens, gain, bias)
+    copies = lax.dynamic_update_slice(copies, jnp.broadcast_to(halo[None], (8, HALO, 256)), (0, 0, 0))
     everyone = lax.all_to_all(copies, TP, 0, 0, tiled=True)
     early = lax.all_gather(early.astype(jnp.float16), SP, axis=0, tiled=True)
 
@@ -115,39 +109,37 @@
     tp = 2 * lax.axis_index("x") + core
     first = jnp.logical_and(lax.axis_index("z") == 0, lax.axis_index("y") == 0)
     rows = HALO + 256
-    copies = [pltpu.make_async_copy(w, held.at[i], sems.at[i]) for i, w in enumerate((w_u, w_outer, w_inner, w_out))]
+    copies = [pltpu.make_async_copy(w_out, held, sems.at[0])]
     for j in range(8):
         at = slice(256 * j, 256 * (j + 1))
-        copies.append(pltpu.make_async_copy(xs.at[j, 0:rows], x.at[:, at], sems.at[4 + j]))
-        copies.append(pltpu.make_async_copy(xs.at[j, rows : rows + 16], tails.at[:, at], sems.at[12 + j]))
-    for copy in copies[4:] + copies[:4]:
-        copy.start()
-    for copy in copies[4:]:
+        copies.append(pltpu.make_async_copy(xs.at[j, 0:rows], x.at[:, at], sems.at[1 + j]))
+        copies.append(pltpu.make_async_copy(xs.at[j, rows : rows + 16], tails.at[:, at], sems.at[9 + j]))
+    for copy in copies[1:] + copies[:1]:
+        copy.start()
+    for copy in copies[1:]:
         copy.wait()
     tail = f32(tails[...])
     table[...] = tail[0:4] + tail[4:8] + tail[8:12]
     alpha = (2.0 * LAYERS) ** 0.25
     kept[:32] = alpha * f32(x[pl.ds(pl.multiple_of(HALO + 32 * tp, 16), 32)])
     kept[32:] = alpha * f32(x[HALO - 8 : HALO])
-    products = []
-    for i in range(3):
-        copies[i].wait()
-        part = jnp.dot(x[...], held[i], preferred_element_type=jnp.float32)
-        products.append(f32(bf(part * (1.0 / IN_UP))))
-    u, outer, inner = products
+    product = lambda w: f32(bf(jnp.dot(x[...], w, preferred_element_type=jnp.float32) * (1.0 / IN_UP)))
+    inner = product(w_inner[...])
+    u = product(w_u[...])
+    outer = product(w_outer[...])
     row = lax.broadcasted_iota(jnp.int32, u.shape, 0)
     z = jnp.where(jnp.logical_and(first, row < HALO), 0.0, inner * u)
     conv = taps[2, 0:1] * z + taps[1, 0:1] * pltpu.roll(z, 1, 0) + taps[0, 0:1] * pltpu.roll(z, 2, 0)
     g[...] = bf(outer * conv)
     half[128:] = g[HALO - 8 : HALO]
-    copies[3].wait()
+    copies[0].wait()
     for target, which in ((sent, 1 - core), (mine, core)):
         for i in range(4):
             half[32 * i : 32 * (i + 1)] = g[pl.ds(pl.multiple_of(HALO + 64 * i + 32 * which, 16), 32)]
         for n in range(4):
             at = slice(512 * n, 512 * (n + 1))
             part = lax.dot_general(
-                half[...], held[3, at], (((1,), (1,)), ((), ())), preferred_element_type=jnp.float32
+                half[...], held[at], (((1,), (1,)), ((), ())), preferred_element_type=jnp.float32
             ) * (1.0 / OUT_UP)
             target[:, at] = part.astype(target.dtype)
 
@@ -156,7 +148,7 @@
     shape = jax.ShapeDtypeStruct
     return pl.pallas_call(
         front_kernel,
-        in_specs=[HBM, HBM, HBM, HBM, HBM, VMEM],
+        in_specs=[HBM, VMEM, VMEM, VMEM, HBM, VMEM],
         out_specs=(VMEM,) * 4,
         out_shape=(
             shape((136, D), jnp.bfloat16),
@@ -169,8 +161,8 @@
             pltpu.VMEM((16, D), jnp.bfloat16),
             pltpu.VMEM((HALO + 256, 256), jnp.bfloat16),
             pltpu.VMEM((136, 256), jnp.bfloat16),
-            pltpu.VMEM((4, D, 256), jnp.bfloat16),
-            pltpu.SemaphoreType.DMA((20,)),
+            pltpu.VMEM((D, 256), jnp.bfloat16),
+            pltpu.SemaphoreType.DMA((17,)),
         ],
         compiler_params=pltpu.CompilerParams(vmem_limit_bytes=49 * 2**20),
         cost_estimate=pl.CostEstimate(flops=1200000000, bytes_accessed=7000000, transcendentals=0),
@@ -225,13 +217,14 @@
     first = jnp.logical_and(lax.axis_index("z") == 0, lax.axis_index("y") == 0)
     step = D // 4
     copies = [
-        pltpu.make_async_copy(w.at[step * i : step * (i + 1)], held.at[step * i : step * (i + 1)], sems.at[i])
-        for i in range(4)
+        pltpu.make_async_copy(w.at[at, 0:768], held.at[at, 0:768], sems.at[i])
+        for i, at in enumerate(pl.ds(step * i, step) for i in range(4))
     ]
+    copies.append(pltpu.make_async_copy(w.at[:, 768:1024], held.at[:, 768:1024], sems.at[4]))
     for copy in copies:
         copy.start()
-    for i, copy in enumerate(copies):
-        copy.wait()
+    for i in range(4):
+        copies[i].wait()
         at = slice(step * i, step * (i + 1))
         for rows, source in ((slice(0, 8), before), (slice(8, 264), x)):
             part = jnp.dot(source[:, at], held[at, :768], preferred_element_type=jnp.float32)
@@ -241,6 +234,7 @@
     z = jnp.where(jnp.logical_and(first, row < 8), 0.0, inner * u)
     conv = taps[2, 1:2] * z + taps[1, 1:2] * pltpu.roll(z, 1, 0) + taps[0, 1:2] * pltpu.roll(z, 2, 0)
     g[...] = bf((outer * conv)[8:])
+    copies[4].wait()
     for target, which in ((sent, 1 - core), (mine, core)):
         for i in range(4):
             half[32 * i : 32 * (i + 1)] = g[pl.ds(pl.multiple_of(64 * i + 32 * which, 16), 32)]
@@ -264,7 +258,7 @@
             pltpu.VMEM((264, 768), jnp.float32),
             pltpu.VMEM((256, 256), jnp.bfloat16),
             pltpu.VMEM((128, 256), jnp.bfloat16),
-            pltpu.SemaphoreType.DMA((4,)),
+            pltpu.SemaphoreType.DMA((5,)),
         ],
         compiler_params=pltpu.CompilerParams(vmem_limit_bytes=50 * 2**20),
         cost_estimate=pl.CostEstimate(flops=1200000000, bytes_accessed=7000000, transcendentals=0),

time: 168 us -> 165 us (0.982)
  Pallas kernels: 13.8 us -> 11.4 us
  blocking collectives: 108 us -> 106 us
  starting transfers between devices: 23.7 us -> 25.5 us
    all_gather x1, blocking collectives: 58.4 us -> 55.4 us  [shards(): early = lax.all_gather(early.astype(jnp.float16), SP, axis=0, tiled=True)]
    pallas_call x3 -> x2, Pallas kernels: 9.11 us -> 6.72 us  [the longest x1 4.01 us: front(): pl.pallas_call(front_kernel, in_specs=[HBM, VMEM, VMEM, VMEM, HBM, VMEM],...]
    ppermute x2, starting transfers between devices: 11 us -> 12.8 us  [shards(): got = lax.ppermute(sent, 'core', [(0, 1), (1, 0)])]
  transfers between devices with their start and end apart: 5 -> 5, of which waited for: 2 -> 2; matrix products, arithmetic and copies ran while one was open for 2% -> 2% of each run, Pallas kernels for 5% -> 3%
where the time goes in v4:
time: 165 us
  blocking collectives  106 us (64%)
  starting transfers between devices  25.5 us (15%)
  between operations  13.5 us (8%)
  Pallas kernels  11.4 us (7%)
  waiting for transfers between devices  3.33 us (2%)
  other arithmetic  2.78 us (2%)
  local copies, waits for them, and re-layouts  2 us (1%)
    all_gather x1, blocking collectives, shards(): early = lax.all_gather(early.astype(jnp.float16), SP, axis=0, tiled=True)  55.4 us
    all_gather x1, blocking collectives, shards(): every = lax.all_gather(own.astype(jnp.float16), TP, axis=0, tiled=True)  15.2 us
    all_to_all x1, blocking collectives, shards(): got = lax.all_to_all(folded(got, mine), 'x', 0, 0, tiled=True)  14.9 us
    ppermute x2, starting transfers between devices, shards(): got = lax.ppermute(sent, 'core', [(0, 1), (1, 0)])  12.8 us
    all_to_all x1, blocking collectives, shards(): lax.all_to_all(bf(f32(got) + f32(mine)).reshape(4, 32, D), 'x', 0, 0, til...  11.7 us
    all_to_all x1, blocking collectives, shards(): lax.all_to_all(last(got, own, table), TP, 0, 0, tiled=True)  8.78 us
    all_to_all x1, starting transfers between devices, shards(): everyone = lax.all_to_all(copies, TP, 0, 0, tiled=True)  8.73 us
    pallas_call x1, Pallas kernels, front(): pl.pallas_call(front_kernel, in_specs=[HBM, VMEM, VMEM, VMEM, HBM, VMEM],...  4.01 us
  transfers between devices with their start and end apart: 5, of which 2 were waited for; matrix products, arithmetic and copies ran while one was open for 2% of the time, Pallas kernels for 3%

profile of v4, /device:TPU:1, one launch (start us, length us, event | category | flops | bytes accessed | tf_op | source)
XLA Modules:
  0.0 164.5 jit_solution(18303677001816947158)
XLA Ops:
  6.5 0.0 all-gather.4.cloned.1.call-start
  6.5 2.7 %shard_map.82 = (bf16[32,1024]{1,0:T(8,128)(2,1)}, bf16[32,1024]{1,0:T(8,128)(2,1)}, bf16[8,288,256]{2,1,0:T(8,128)(2,1)}) custom-call(bf16[2,32,256]{2,1,0:T(8,128)(2,1)} %value.1, bf16[2,32,256]{2,1,0:T(8,128)(2,1)} %outer.1, bf16[2,32,256]{2,1,0:T(8,128)(2,1)} %inner.1, bf16[2,32,256]{2,1,0:T(8,128)(2,1)} %bitcast.8, bf16[256,256]{1,0:T(8,128)(2,1)} %tokens.1, ...), custom_call_target="tpu_custom_call" | custom-call | flops 2000000 | bytes 1700000 | tf_op jit(solution)/shard_map/pallas_call | solution.py:64
  9.3 0.0 all-gather.4.cloned.1.call-update
  9.3 0.7 slice.15
  10.0 4.0 %collective-permute-start = (bf16[16,256]{1,0:T(8,128)(2,1)S(1)}, bf16[16,256]{1,0:T(8,128)(2,1)S(1)}, u32[]{:S(2)}, u32[]{:S(2)}) collective-permute-start(bf16[16,256]{1,0:T(8,128)(2,1)S(1)} %slice.15), channel_id=1, source_target_pairs={{0,8},{8,16},{16,24},{24,32},{32,40},{40,48},{48,56},{56,64},{64,7... | collective-permute-start | bytes 24584 | tf_op jit(solution)/shard_map/ppermute | solution.py:88
  14.0 0.9 convert_element_type.30
  14.9 0.0 collective-permute-done
  14.9 0.6 broadcast_dynamic-update-slice_fusion
  15.5 8.7 %all-to-all-start = ((bf16[8,288,256]{2,1,0:T(8,128)(2,1)}), bf16[8,288,256]{2,1,0:T(8,128)(2,1)}, u32[]{:S(2)}, u32[]{:S(2)}) async-start(bf16[8,288,256]{2,1,0:T(8,128)(2,1)} %broadcast_dynamic-update-slice_fusion), calls=%async_computation | async-start | bytes 2359296 | tf_op jit(solution)/shard_map/all_to_all | solution.py:92
  24.2 55.4 %all-gather.5 = f16[2048,1024]{1,0:T(8,128)(2,1)S(1)} all-gather(f16[32,1024]{1,0:T(8,128)(2,1)S(1)} %convert_element_type.30), channel_id=1, replica_groups=mesh['z'=8,'y'=8,'x'=4,'core'=2] {'z','y'}, dimensions={0}, use_global_device_ids=true | all-gather | bytes 4259840 | tf_op jit(solution)/shard_map/all_gather | solution.py:93
  79.6 0.0 copy-start
  79.6 1.6 slice_convert_fusion
  81.2 0.0 all-to-all-done.xs
  81.2 0.0 copy-done
  81.2 4.0 %shard_map.83 = (bf16[136,2048]{1,0:T(8,128)(2,1)S(1)}, bf16[136,2048]{1,0:T(8,128)(2,1)S(1)}, f32[40,2048]{1,0:T(8,128)S(1)}, f32[4,2048]{1,0:T(4,128)S(1)}) custom-call(bf16[8,288,256]{2,1,0:T(8,128)(2,1)} %all-to-all-done.xs, bf16[2048,256]{1,0:T(8,128)(2,1)S(1)} %get-tuple-element.30.w_u, bf16[2048,256]{1,0:T(8,128)(2,1)S(1)} %get-tuple-element.29.w_outer, ...), custom_call_target="tpu_custom_call" | custom-call | flops 1200000000 | bytes 7000000 | tf_op jit(solution)/shard_map/pallas_call | solution.py:149
  85.2 10.7 %collective-permute-start.1 = (bf16[136,2048]{1,0:T(8,128)(2,1)S(1)}, bf16[136,2048]{1,0:T(8,128)(2,1)S(1)}, u32[]{:S(2)}, u32[]{:S(2)}) collective-permute-start(bf16[136,2048]{1,0:T(8,128)(2,1)S(1)} %get-tuple-element.18), channel_id=1, source_target_pairs={{0,1},{1,0},{2,3},{3,2},{4,5},{5,4},{6,7},{7,6},{8,9},{9,8},{10,11... | collective-permute-start | bytes 1671176 | tf_op jit(solution)/shard_map/ppermute | solution.py:96
  96.0 1.6 collective-permute-done.1.got
  97.5 0.3 shard_map.84
  97.8 14.9 %all_to_all.20.got = bf16[4,32,2176]{2,1,0:T(8,128)(2,1)S(1)} all-to-all(bf16[4,32,2176]{2,1,0:T(8,128)(2,1)S(1)} %shard_map.84), channel_id=1, replica_groups=mesh['z'=8,'y'=8,'x'=4,'core'=2] {'x'}, dimensions={0} | all-to-all | bytes 1114112 | tf_op jit(solution)/shard_map/all_to_all | solution.py:97
  112.8 0.3 shard_map.85
  113.1 15.2 %all-gather.6 = f16[256,2048]{1,0:T(8,128)(2,1)S(1)} all-gather(f16[32,2048]{1,0:T(8,128)(2,1)S(1)} %convert_element_type.35), channel_id=1, replica_groups=mesh['z'=8,'y'=8,'x'=4,'core'=2] {'x','core'}, dimensions={0}, use_global_device_ids=true | all-gather | bytes 1179648 | tf_op jit(solution)/shard_map/all_gather | solution.py:99
  128.3 0.1 convert_element_type.36.x
  128.5 0.0 all-gather.4.cloned.1.call-done.w
  128.5 3.8 %shard_map.86 = (bf16[128,2048]{1,0:T(8,128)(2,1)S(1)}, bf16[128,2048]{1,0:T(8,128)(2,1)S(1)}) custom-call(bf16[256,2048]{1,0:T(8,128)(2,1)S(1)} %convert_element_type.36.x, bf16[8,2048]{1,0:T(8,128)(2,1)S(1)} %get-tuple-element.23.before, bf16[2048,1024]{1,0:T(8,128)(2,1)} %all-gather.4.cloned.1.call-done.w, f32[3,2,256]{2,1,0:T(2,128)S(1)} %bitcast.5), custom_call_target="tpu_custom_call" | custom-call | flops 1200000000 | bytes 7000000 | tf_op jit(solution)/shard_map/pallas_call | solution.py:251
  132.3 2.1 %collective-permute-start.2 = (bf16[128,2048]{1,0:T(8,128)(2,1)S(1)}, bf16[128,2048]{1,0:T(8,128)(2,1)S(1)}, u32[]{:S(2)}, u32[]{:S(2)}) collective-permute-start(bf16[128,2048]{1,0:T(8,128)(2,1)S(1)} %get-tuple-element.25), channel_id=1, source_target_pairs={{0,1},{1,0},{2,3},{3,2},{4,5},{5,4},{6,7},{7,6},{8,9},{9,8},{10,11... | collective-permute-start | bytes 1572872 | tf_op jit(solution)/shard_map/ppermute | solution.py:102
  134.4 1.7 %collective-permute-done.2 = bf16[128,2048]{1,0:T(8,128)(2,1)S(1)} collective-permute-done((bf16[128,2048]{1,0:T(8,128)(2,1)S(1)}, bf16[128,2048]{1,0:T(8,128)(2,1)S(1)}, u32[]{:S(2)}, u32[]{:S(2)}) %collective-permute-start.2) | collective-permute-done | bytes 524320 | tf_op jit(solution)/shard_map/ppermute | solution.py:102
  136.1 0.1 add_convert_fusion
  136.3 11.7 %all_to_all.21.got = bf16[4,32,2048]{2,1,0:T(8,128)(2,1)S(1)} all-to-all(bf16[4,32,2048]{2,1,0:T(8,128)(2,1)S(1)} %bitcast.6), channel_id=1, replica_groups=mesh['z'=8,'y'=8,'x'=4,'core'=2] {'x'}, dimensions={0} | all-to-all | bytes 1048576 | tf_op jit(solution)/shard_map/all_to_all | solution.py:103
  147.9 0.3 shard_map.87
  148.3 8.8 %all_to_all.22 = bf16[8,32,256]{2,1,0:T(8,128)(2,1)S(1)} all-to-all(bf16[8,32,256]{2,1,0:T(8,128)(2,1)S(1)} %shard_map.87), channel_id=1, replica_groups=mesh['z'=8,'y'=8,'x'=4,'core'=2] {'x','core'}, dimensions={0} | all-to-all | bytes 262144 | tf_op jit(solution)/shard_map/all_to_all | solution.py:104
  157.0 0.7 copy.11
  (1 shorter events, 0.0 us)
Async XLA Ops:
  6.5 122.0 %all-gather.4.cloned.1.call-start = ((), (), s32[]{:S(2)}) async-start(), calls=%async_computation.4 | async-start | bytes 4259840 | tf_op jit(solution)/shard_map/all_gather | solution.py:90
  10.0 4.9 %collective-permute-start = (bf16[16,256]{1,0:T(8,128)(2,1)S(1)}, bf16[16,256]{1,0:T(8,128)(2,1)S(1)}, u32[]{:S(2)}, u32[]{:S(2)}) collective-permute-start(bf16[16,256]{1,0:T(8,128)(2,1)S(1)} %slice.15), channel_id=1, source_target_pairs={{0,8},{8,16},{16,24},{24,32},{32,40},{40,48},{48,56},{56,64},{64,7... | collective-permute-start | bytes 24584 | tf_op jit(solution)/shard_map/ppermute | solution.py:88
  15.5 65.7 %all-to-all-start = ((bf16[8,288,256]{2,1,0:T(8,128)(2,1)}), bf16[8,288,256]{2,1,0:T(8,128)(2,1)}, u32[]{:S(2)}, u32[]{:S(2)}) async-start(bf16[8,288,256]{2,1,0:T(8,128)(2,1)} %broadcast_dynamic-update-slice_fusion), calls=%async_computation | async-start | bytes 2359296 | tf_op jit(solution)/shard_map/all_to_all | solution.py:92
  79.6 1.7 %copy-start = (f32[2,3,256]{2,0,1:T(2,128)S(1)}, f32[2,3,256]{2,0,1:T(2,128)}, u32[]{:S(2)}) copy-start(f32[2,3,256]{2,0,1:T(2,128)} %param.12) | copy-start | bytes 18436
  85.2 12.3 %collective-permute-start.1 = (bf16[136,2048]{1,0:T(8,128)(2,1)S(1)}, bf16[136,2048]{1,0:T(8,128)(2,1)S(1)}, u32[]{:S(2)}, u32[]{:S(2)}) collective-permute-start(bf16[136,2048]{1,0:T(8,128)(2,1)S(1)} %get-tuple-element.18), channel_id=1, source_target_pairs={{0,1},{1,0},{2,3},{3,2},{4,5},{5,4},{6,7},{7,6},{8,9},{9,8},{10,11... | collective-permute-start | bytes 1671176 | tf_op jit(solution)/shard_map/ppermute | solution.py:96
  132.3 3.8 %collective-permute-start.2 = (bf16[128,2048]{1,0:T(8,128)(2,1)S(1)}, bf16[128,2048]{1,0:T(8,128)(2,1)S(1)}, u32[]{:S(2)}, u32[]{:S(2)}) collective-permute-start(bf16[128,2048]{1,0:T(8,128)(2,1)S(1)} %get-tuple-element.25), channel_id=1, source_target_pairs={{0,1},{1,0},{2,3},{3,2},{4,5},{5,4},{6,7},{7,6},{8,9},{9,8},{10,11... | collective-permute-start | bytes 1572872 | tf_op jit(solution)/shard_map/ppermute | solution.py:102
Sparse Core Ops, SparseCore 0:
  10.4 91.5 all-gather.3

commit v5 on v4

--- a/solution.py
+++ b/solution.py
@@ -1,3 +1,5 @@
+import functools
+
 import jax
 import jax.numpy as jnp
 from jax import lax
@@ -92,56 +94,66 @@
     everyone = lax.all_to_all(copies, TP, 0, 0, tiled=True)
     early = lax.all_gather(early.astype(jnp.float16), SP, axis=0, tiled=True)
 
-    sent, mine, kept, table = front(everyone, [bf(early[:, 256 * i : 256 * (i + 1)]) for i in range(4)], taps)
+    weights = [bf(early[:, 256 * i : 256 * (i + 1)]) for i in range(4)]
+    sent, half, kept, table = front(everyone, weights, taps)
     got = lax.ppermute(sent, "core", [(0, 1), (1, 0)])
+    mine = own_product(half, weights[3], 0, 1.0 / OUT_UP, 49)
     got = lax.all_to_all(folded(got, mine), "x", 0, 0, tiled=True)
     own, before = middle(got, kept, table)
     every = lax.all_gather(own.astype(jnp.float16), TP, axis=0, tiled=True)
 
-    sent, mine = rear(bf(every), before, late, taps)
+    sent, half = rear(bf(every), before, late, taps)
     got = lax.ppermute(sent, "core", [(0, 1), (1, 0)])
+    mine = own_product(half, late, 768, 1.0, 52)
     got = lax.all_to_all(bf(f32(got) + f32(mine)).reshape(4, 32, D), "x", 0, 0, tiled=True)
     return lax.all_to_all(last(got, own, table), TP, 0, 0, tiled=True).reshape(256, 256)
 
 
-def front_kernel(xs, w_u, w_outer, w_inner, w_out, taps, sent, mine, kept, table, x, tails, g, half, held, sems):
+def out_product(rows, w_out, down, target):
+    for n in range(4):
+        at = slice(512 * n, 512 * (n + 1))
+        part = lax.dot_general(rows, w_out[at], (((1,), (1,)), ((), ())), preferred_element_type=jnp.float32)
+        target[:, at] = bf(part * down)
+
+
+def front_kernel(xs, w_u, w_outer, w_inner, w_out, taps, sent, own, kept, table, x, tails, g, half, held, sems):
     core = lax.axis_index("core")
     tp = 2 * lax.axis_index("x") + core
     first = jnp.logical_and(lax.axis_index("z") == 0, lax.axis_index("y") == 0)
     rows = HALO + 256
-    copies = [pltpu.make_async_copy(w_out, held, sems.at[0])]
+    blocks, ends = [], []
     for j in range(8):
         at = slice(256 * j, 256 * (j + 1))
-        copies.append(pltpu.make_async_copy(xs.at[j, 0:rows], x.at[:, at], sems.at[1 + j]))
-        copies.append(pltpu.make_async_copy(xs.at[j, rows : rows + 16], tails.at[:, at], sems.at[9 + j]))
-    for copy in copies[1:] + copies[:1]:
+        blocks.append(pltpu.make_async_copy(xs.at[j, 0:rows], x.at[:, at], sems.at[j]))
+        ends.append(pltpu.make_async_copy(xs.at[j, rows : rows + 16], tails.at[:, at], sems.at[8 + j]))
+    weight = pltpu.make_async_copy(w_out, held, sems.at[16])
+    for copy in blocks + [weight] + ends:
         copy.start()
-    for copy in copies[1:]:
-        copy.wait()
-    tail = f32(tails[...])
-    table[...] = tail[0:4] + tail[4:8] + tail[8:12]
-    alpha = (2.0 * LAYERS) ** 0.25
-    kept[:32] = alpha * f32(x[pl.ds(pl.multiple_of(HALO + 32 * tp, 16), 32)])
-    kept[32:] = alpha * f32(x[HALO - 8 : HALO])
-    product = lambda w: f32(bf(jnp.dot(x[...], w, preferred_element_type=jnp.float32) * (1.0 / IN_UP)))
-    inner = product(w_inner[...])
-    u = product(w_u[...])
-    outer = product(w_outer[...])
+    sums = [0.0, 0.0, 0.0]
+    for part in range(2):
+        for copy in blocks[4 * part : 4 * (part + 1)]:
+            copy.wait()
+        at = slice(1024 * part, 1024 * (part + 1))
+        for i, w in enumerate((w_u, w_outer, w_inner)):
+            sums[i] = sums[i] + jnp.dot(x[:, at], w[at], preferred_element_type=jnp.float32)
+    u, outer, inner = (f32(bf(total * (1.0 / IN_UP))) for total in sums)
     row = lax.broadcasted_iota(jnp.int32, u.shape, 0)
     z = jnp.where(jnp.logical_and(first, row < HALO), 0.0, inner * u)
     conv = taps[2, 0:1] * z + taps[1, 0:1] * pltpu.roll(z, 1, 0) + taps[0, 0:1] * pltpu.roll(z, 2, 0)
     g[...] = bf(outer * conv)
-    half[128:] = g[HALO - 8 : HALO]
-    copies[0].wait()
-    for target, which in ((sent, 1 - core), (mine, core)):
+    for target, which in ((half, 1 - core), (own, core)):
+        target[128:] = g[HALO - 8 : HALO]
         for i in range(4):
-            half[32 * i : 32 * (i + 1)] = g[pl.ds(pl.multiple_of(HALO + 64 * i + 32 * which, 16), 32)]
-        for n in range(4):
-            at = slice(512 * n, 512 * (n + 1))
-            part = lax.dot_general(
-                half[...], held[at], (((1,), (1,)), ((), ())), preferred_element_type=jnp.float32
-            ) * (1.0 / OUT_UP)
-            target[:, at] = part.astype(target.dtype)
+            target[32 * i : 32 * (i + 1)] = g[pl.ds(pl.multiple_of(HALO + 64 * i + 32 * which, 16), 32)]
+    weight.wait()
+    out_product(half[...], held, 1.0 / OUT_UP, sent)
+    alpha = (2.0 * LAYERS) ** 0.25
+    kept[:32] = alpha * f32(x[pl.ds(pl.multiple_of(HALO + 32 * tp, 16), 32)])
+    kept[32:] = alpha * f32(x[HALO - 8 : HALO])
+    for copy in ends:
+        copy.wait()
+    tail = f32(tails[...])
+    table[...] = tail[0:4] + tail[4:8] + tail[8:12]
 
 
 def front(xs, weights, taps):
@@ -152,7 +164,7 @@
         out_specs=(VMEM,) * 4,
         out_shape=(
             shape((136, D), jnp.bfloat16),
-            shape((136, D), jnp.bfloat16),
+            shape((136, 256), jnp.bfloat16),
             shape((40, D), jnp.float32),
             shape((4, D), jnp.float32),
         ),
@@ -169,6 +181,25 @@
     )(xs, *weights, taps)
 
 
+def own_kernel(column, down, rows, w, mine, held, sem):
+    copy = pltpu.make_async_copy(w.at[:, column : column + 256], held, sem.at[0])
+    copy.start()
+    copy.wait()
+    out_product(rows[...], held, down, mine)
+
+
+def own_product(rows, w, column, down, limit):
+    return pl.pallas_call(
+        functools.partial(own_kernel, column, down),
+        in_specs=[VMEM, HBM],
+        out_specs=VMEM,
+        out_shape=jax.ShapeDtypeStruct((rows.shape[0], D), jnp.bfloat16),
+        scratch_shapes=[pltpu.VMEM((D, 256), jnp.bfloat16), pltpu.SemaphoreType.DMA((1,))],
+        compiler_params=pltpu.CompilerParams(vmem_limit_bytes=limit * 2**20),
+        cost_estimate=pl.CostEstimate(flops=800000000, bytes_accessed=2000000, transcendentals=0),
+    )(rows, w)
+
+
 def fold_kernel(got, mine, out, strip):
     total = f32(got[...]) + f32(mine[...])
     for i in range(4):
@@ -212,7 +243,7 @@
     )(got, kept, table)
 
 
-def rear_kernel(x, before, w, taps, sent, mine, held, acc, g, half, sems):
+def rear_kernel(x, before, w, taps, sent, own, held, acc, g, half, sems):
     core = lax.axis_index("core")
     first = jnp.logical_and(lax.axis_index("z") == 0, lax.axis_index("y") == 0)
     step = D // 4
@@ -234,16 +265,11 @@
     z = jnp.where(jnp.logical_and(first, row < 8), 0.0, inner * u)
     conv = taps[2, 1:2] * z + taps[1, 1:2] * pltpu.roll(z, 1, 0) + taps[0, 1:2] * pltpu.roll(z, 2, 0)
     g[...] = bf((outer * conv)[8:])
+    for target, which in ((half, 1 - core), (own, core)):
+        for i in range(4):
+            target[32 * i : 32 * (i + 1)] = g[pl.ds(pl.multiple_of(64 * i + 32 * which, 16), 32)]
     copies[4].wait()
-    for target, which in ((sent, 1 - core), (mine, core)):
-        for i in range(4):
-            half[32 * i : 32 * (i + 1)] = g[pl.ds(pl.multiple_of(64 * i + 32 * which, 16), 32)]
-        for n in range(4):
-            at = slice(512 * n, 512 * (n + 1))
-            part = lax.dot_general(
-                half[...], held[at, 768:], (((1,), (1,)), ((), ())), preferred_element_type=jnp.float32
-            )
-            target[:, at] = part.astype(target.dtype)
+    out_product(half[...], held.at[:, 768:1024], 1.0, sent)
 
 
 def rear(x, before, w, taps):
@@ -252,7 +278,7 @@
         rear_kernel,
         in_specs=[VMEM, VMEM, HBM, VMEM],
         out_specs=(VMEM, VMEM),
-        out_shape=(shape((128, D), jnp.bfloat16),) * 2,
+        out_shape=(shape((128, D), jnp.bfloat16), shape((128, 256), jnp.bfloat16)),
         scratch_shapes=[
             pltpu.VMEM((D, 1024), jnp.bfloat16),
             pltpu.VMEM((264, 768), jnp.float32),

time: 165 us -> 165 us (level)
  waiting for transfers between devices: 3.33 us -> 1.02 us
  Pallas kernels: 11.4 us -> 13.1 us
    ppermute x2, waiting for transfers between devices: 3.29 us -> 0.98 us  [shards(): got = lax.ppermute(sent, 'core', [(0, 1), (1, 0)])]
    pallas_call x0 -> x2, Pallas kernels: none -> 2.29 us  [own_product(): pl.pallas_call(functools.partial(own_kernel, column, down), in_specs=[VME...]
  transfers between devices with their start and end apart: 5 -> 5, of which waited for: 2 -> 1; matrix products, arithmetic and copies ran while one was open for 2% -> 2% of each run, Pallas kernels for 3% -> 4%
where the time goes in v5:
time: 165 us; the launch traced here: 164 us
  blocking collectives  106 us (64%)
  starting transfers between devices  25.4 us (15%)
  between operations  13.5 us (8%)
  Pallas kernels  13.1 us (8%)
  other arithmetic  2.78 us (2%)
  local copies, waits for them, and re-layouts  2 us (1%)
    all_gather x1, blocking collectives, shards(): early = lax.all_gather(early.astype(jnp.float16), SP, axis=0, tiled=True)  55.5 us
    all_gather x1, blocking collectives, shards(): every = lax.all_gather(own.astype(jnp.float16), TP, axis=0, tiled=True)  15.2 us
    all_to_all x1, blocking collectives, shards(): got = lax.all_to_all(folded(got, mine), 'x', 0, 0, tiled=True)  15.2 us
    ppermute x2, starting transfers between devices, shards(): got = lax.ppermute(sent, 'core', [(0, 1), (1, 0)])  12.6 us
    all_to_all x1, blocking collectives, shards(): lax.all_to_all(bf(f32(got) + f32(mine)).reshape(4, 32, D), 'x', 0, 0, til...  11.5 us
    all_to_all x1, blocking collectives, shards(): lax.all_to_all(last(got, own, table), TP, 0, 0, tiled=True)  8.97 us
    all_to_all x1, starting transfers between devices, shards(): everyone = lax.all_to_all(copies, TP, 0, 0, tiled=True)  8.74 us
    ppermute x1, starting transfers between devices, shards(): halo = lax.ppermute(tokens[-HALO:], SP, [(i, i + 1) for i in range(63)])  4.01 us
  transfers between devices with their start and end apart: 5, of which 1 were waited for; matrix products, arithmetic and copies ran while one was open for 2% of the time, Pallas kernels for 4%

profile of v5, /device:TPU:1, one launch (start us, length us, event | category | flops | bytes accessed | tf_op | source)
XLA Modules:
  0.0 164.1 jit_solution(1162021865315598037)
XLA Ops:
  6.5 0.0 all-gather.4.cloned.1.call-start
  6.5 2.7 %shard_map.82 = (bf16[32,1024]{1,0:T(8,128)(2,1)}, bf16[32,1024]{1,0:T(8,128)(2,1)}, bf16[8,288,256]{2,1,0:T(8,128)(2,1)}) custom-call(bf16[2,32,256]{2,1,0:T(8,128)(2,1)} %value.1, bf16[2,32,256]{2,1,0:T(8,128)(2,1)} %outer.1, bf16[2,32,256]{2,1,0:T(8,128)(2,1)} %inner.1, bf16[2,32,256]{2,1,0:T(8,128)(2,1)} %bitcast.8, bf16[256,256]{1,0:T(8,128)(2,1)} %tokens.1, ...), custom_call_target="tpu_custom_call" | custom-call | flops 2000000 | bytes 1700000 | tf_op jit(solution)/shard_map/pallas_call | solution.py:66
  9.2 0.0 all-gather.4.cloned.1.call-update
  9.3 0.7 slice.15
  10.0 4.0 %collective-permute-start = (bf16[16,256]{1,0:T(8,128)(2,1)S(1)}, bf16[16,256]{1,0:T(8,128)(2,1)S(1)}, u32[]{:S(2)}, u32[]{:S(2)}) collective-permute-start(bf16[16,256]{1,0:T(8,128)(2,1)S(1)} %slice.15), channel_id=1, source_target_pairs={{0,8},{8,16},{16,24},{24,32},{32,40},{40,48},{48,56},{56,64},{64,7... | collective-permute-start | bytes 24584 | tf_op jit(solution)/shard_map/ppermute | solution.py:90
  14.0 0.9 convert_element_type.30
  14.8 0.0 collective-permute-done
  14.8 0.6 broadcast_dynamic-update-slice_fusion
  15.5 8.7 %all-to-all-start = ((bf16[8,288,256]{2,1,0:T(8,128)(2,1)}), bf16[8,288,256]{2,1,0:T(8,128)(2,1)}, u32[]{:S(2)}, u32[]{:S(2)}) async-start(bf16[8,288,256]{2,1,0:T(8,128)(2,1)} %broadcast_dynamic-update-slice_fusion), calls=%async_computation | async-start | bytes 2359296 | tf_op jit(solution)/shard_map/all_to_all | solution.py:94
  24.2 55.5 %all-gather.5 = f16[2048,1024]{1,0:T(8,128)(2,1)S(1)} all-gather(f16[32,1024]{1,0:T(8,128)(2,1)S(1)} %convert_element_type.30), channel_id=1, replica_groups=mesh['z'=8,'y'=8,'x'=4,'core'=2] {'z','y'}, dimensions={0}, use_global_device_ids=true | all-gather | bytes 4259840 | tf_op jit(solution)/shard_map/all_gather | solution.py:95
  79.7 1.6 slice_convert_fusion
  81.3 0.0 all-to-all-done.xs
  81.3 0.0 copy-done.1
  81.3 3.7 %shard_map.83 = (bf16[136,2048]{1,0:T(8,128)(2,1)S(1)}, bf16[136,256]{1,0:T(8,128)(2,1)S(1)}, f32[40,2048]{1,0:T(8,128)S(1)}, f32[4,2048]{1,0:T(4,128)S(1)}) custom-call(bf16[8,288,256]{2,1,0:T(8,128)(2,1)} %all-to-all-done.xs, bf16[2048,256]{1,0:T(8,128)(2,1)S(1)} %get-tuple-element.30.w_u, bf16[2048,256]{1,0:T(8,128)(2,1)S(1)} %get-tuple-element.29.w_outer, ...), custom_call_target="tpu_custom_call" | custom-call | flops 1200000000 | bytes 7000000 | tf_op jit(solution)/shard_map/pallas_call | solution.py:161
  85.1 10.6 %collective-permute-start.1 = (bf16[136,2048]{1,0:T(8,128)(2,1)S(1)}, bf16[136,2048]{1,0:T(8,128)(2,1)S(1)}, u32[]{:S(2)}, u32[]{:S(2)}) collective-permute-start(bf16[136,2048]{1,0:T(8,128)(2,1)S(1)} %get-tuple-element.18), channel_id=1, source_target_pairs={{0,1},{1,0},{2,3},{3,2},{4,5},{5,4},{6,7},{7,6},{8,9},{9,8},{10,11... | collective-permute-start | bytes 1671176 | tf_op jit(solution)/shard_map/ppermute | solution.py:99
  95.7 0.6 shard_map.84.mine
  96.2 1.0 collective-permute-done.1.got
  97.2 0.3 shard_map.85
  97.5 15.2 %all_to_all.20.got = bf16[4,32,2176]{2,1,0:T(8,128)(2,1)S(1)} all-to-all(bf16[4,32,2176]{2,1,0:T(8,128)(2,1)S(1)} %shard_map.85), channel_id=1, replica_groups=mesh['z'=8,'y'=8,'x'=4,'core'=2] {'x'}, dimensions={0} | all-to-all | bytes 1114112 | tf_op jit(solution)/shard_map/all_to_all | solution.py:101
  112.7 0.3 shard_map.86
  113.0 15.2 %all-gather.6 = f16[256,2048]{1,0:T(8,128)(2,1)S(1)} all-gather(f16[32,2048]{1,0:T(8,128)(2,1)S(1)} %convert_element_type.35), channel_id=1, replica_groups=mesh['z'=8,'y'=8,'x'=4,'core'=2] {'x','core'}, dimensions={0}, use_global_device_ids=true | all-gather | bytes 1179648 | tf_op jit(solution)/shard_map/all_gather | solution.py:103
  128.2 0.1 convert_element_type.36.x
  128.4 0.0 all-gather.4.cloned.1.call-done.w
  128.4 3.5 %shard_map.87 = (bf16[128,2048]{1,0:T(8,128)(2,1)S(1)}, bf16[128,256]{1,0:T(8,128)(2,1)S(1)}) custom-call(bf16[256,2048]{1,0:T(8,128)(2,1)S(1)} %convert_element_type.36.x, bf16[8,2048]{1,0:T(8,128)(2,1)S(1)} %get-tuple-element.23.before, bf16[2048,1024]{1,0:T(8,128)(2,1)} %all-gather.4.cloned.1.call-done.w, f32[3,2,256]{2,1,0:T(2,128)S(1)} %bitcast.5), custom_call_target="tpu_custom_call" | custom-call | flops 1200000000 | bytes 7000000 | tf_op jit(solution)/shard_map/pallas_call | solution.py:277
  131.9 2.1 %collective-permute-start.2 = (bf16[128,2048]{1,0:T(8,128)(2,1)S(1)}, bf16[128,2048]{1,0:T(8,128)(2,1)S(1)}, u32[]{:S(2)}, u32[]{:S(2)}) collective-permute-start(bf16[128,2048]{1,0:T(8,128)(2,1)S(1)} %get-tuple-element.25), channel_id=1, source_target_pairs={{0,1},{1,0},{2,3},{3,2},{4,5},{5,4},{6,7},{7,6},{8,9},{9,8},{10,11... | collective-permute-start | bytes 1572872 | tf_op jit(solution)/shard_map/ppermute | solution.py:106
  134.0 1.7 %shard_map.88 = bf16[128,2048]{1,0:T(8,128)(2,1)S(1)} custom-call(bf16[128,256]{1,0:T(8,128)(2,1)S(1)} %get-tuple-element.26.rows, bf16[2048,1024]{1,0:T(8,128)(2,1)} %all-gather.4.cloned.1.call-done.w), custom_call_target="tpu_custom_call" | custom-call | flops 800000000 | bytes 2000000 | tf_op jit(solution)/shard_map/pallas_call | solution.py:192
  135.7 0.0 collective-permute-done.2
  135.7 0.1 add_convert_fusion
  135.9 11.5 %all_to_all.21.got = bf16[4,32,2048]{2,1,0:T(8,128)(2,1)S(1)} all-to-all(bf16[4,32,2048]{2,1,0:T(8,128)(2,1)S(1)} %bitcast.6), channel_id=1, replica_groups=mesh['z'=8,'y'=8,'x'=4,'core'=2] {'x'}, dimensions={0} | all-to-all | bytes 1048576 | tf_op jit(solution)/shard_map/all_to_all | solution.py:108
  147.4 0.3 shard_map.89
  147.7 9.0 %all_to_all.22 = bf16[8,32,256]{2,1,0:T(8,128)(2,1)S(1)} all-to-all(bf16[8,32,256]{2,1,0:T(8,128)(2,1)S(1)} %shard_map.89), channel_id=1, replica_groups=mesh['z'=8,'y'=8,'x'=4,'core'=2] {'x','core'}, dimensions={0} | all-to-all | bytes 262144 | tf_op jit(solution)/shard_map/all_to_all | solution.py:109
  156.6 0.7 copy.11
  (4 shorter events, 0.0 us)
Async XLA Ops:
  6.5 121.9 %all-gather.4.cloned.1.call-start = ((), (), s32[]{:S(2)}) async-start(), calls=%async_computation.4 | async-start | bytes 4259840 | tf_op jit(solution)/shard_map/all_gather | solution.py:92
  10.0 4.9 %collective-permute-start = (bf16[16,256]{1,0:T(8,128)(2,1)S(1)}, bf16[16,256]{1,0:T(8,128)(2,1)S(1)}, u32[]{:S(2)}, u32[]{:S(2)}) collective-permute-start(bf16[16,256]{1,0:T(8,128)(2,1)S(1)} %slice.15), channel_id=1, source_target_pairs={{0,8},{8,16},{16,24},{24,32},{32,40},{40,48},{48,56},{56,64},{64,7... | collective-permute-start | bytes 24584 | tf_op jit(solution)/shard_map/ppermute | solution.py:90
  15.5 65.8 %all-to-all-start = ((bf16[8,288,256]{2,1,0:T(8,128)(2,1)}), bf16[8,288,256]{2,1,0:T(8,128)(2,1)}, u32[]{:S(2)}, u32[]{:S(2)}) async-start(bf16[8,288,256]{2,1,0:T(8,128)(2,1)} %broadcast_dynamic-update-slice_fusion), calls=%async_computation | async-start | bytes 2359296 | tf_op jit(solution)/shard_map/all_to_all | solution.py:94
  79.7 1.6 %copy-start.1 = (f32[2,3,256]{2,0,1:T(2,128)S(1)}, f32[2,3,256]{2,0,1:T(2,128)}, u32[]{:S(2)}) copy-start(f32[2,3,256]{2,0,1:T(2,128)} %param.12) | copy-start | bytes 18436
  81.3 14.3 %copy-start = (bf16[2048,256]{1,0:T(8,128)(2,1)S(1)}, bf16[2048,256]{1,0:T(8,128)(2,1)}, u32[]{:S(2)}) copy-start(bf16[2048,256]{1,0:T(8,128)(2,1)} %get-tuple-element.27.w_out.w) | copy-start | bytes 3145732
  85.1 12.2 %collective-permute-start.1 = (bf16[136,2048]{1,0:T(8,128)(2,1)S(1)}, bf16[136,2048]{1,0:T(8,128)(2,1)S(1)}, u32[]{:S(2)}, u32[]{:S(2)}) collective-permute-start(bf16[136,2048]{1,0:T(8,128)(2,1)S(1)} %get-tuple-element.18), channel_id=1, source_target_pairs={{0,1},{1,0},{2,3},{3,2},{4,5},{5,4},{6,7},{7,6},{8,9},{9,8},{10,11... | collective-permute-start | bytes 1671176 | tf_op jit(solution)/shard_map/ppermute | solution.py:99
  131.9 3.8 %collective-permute-start.2 = (bf16[128,2048]{1,0:T(8,128)(2,1)S(1)}, bf16[128,2048]{1,0:T(8,128)(2,1)S(1)}, u32[]{:S(2)}, u32[]{:S(2)}) collective-permute-start(bf16[128,2048]{1,0:T(8,128)(2,1)S(1)} %get-tuple-element.25), channel_id=1, source_target_pairs={{0,1},{1,0},{2,3},{3,2},{4,5},{5,4},{6,7},{7,6},{8,9},{9,8},{10,11... | collective-permute-start | bytes 1572872 | tf_op jit(solution)/shard_map/ppermute | solution.py:106
Sparse Core Ops, SparseCore 0:
  10.4 91.4 all-gather.3

commit v6 on v5

--- a/solution.py
+++ b/solution.py
@@ -95,9 +95,9 @@
     early = lax.all_gather(early.astype(jnp.float16), SP, axis=0, tiled=True)
 
     weights = [bf(early[:, 256 * i : 256 * (i + 1)]) for i in range(4)]
-    sent, half, kept, table = front(everyone, weights, taps)
+    sent, half = front(everyone, weights, taps)
     got = lax.ppermute(sent, "core", [(0, 1), (1, 0)])
-    mine = own_product(half, weights[3], 0, 1.0 / OUT_UP, 49)
+    mine, kept, table = aside(half, weights[3], everyone)
     got = lax.all_to_all(folded(got, mine), "x", 0, 0, tiled=True)
     own, before = middle(got, kept, table)
     every = lax.all_gather(own.astype(jnp.float16), TP, axis=0, tiled=True)
@@ -116,23 +116,22 @@
         target[:, at] = bf(part * down)
 
 
-def front_kernel(xs, w_u, w_outer, w_inner, w_out, taps, sent, own, kept, table, x, tails, g, half, held, sems):
+def front_kernel(xs, w_u, w_outer, w_inner, w_out, taps, sent, own, x, g, half, held, sems):
     core = lax.axis_index("core")
-    tp = 2 * lax.axis_index("x") + core
     first = jnp.logical_and(lax.axis_index("z") == 0, lax.axis_index("y") == 0)
     rows = HALO + 256
-    blocks, ends = [], []
-    for j in range(8):
-        at = slice(256 * j, 256 * (j + 1))
-        blocks.append(pltpu.make_async_copy(xs.at[j, 0:rows], x.at[:, at], sems.at[j]))
-        ends.append(pltpu.make_async_copy(xs.at[j, rows : rows + 16], tails.at[:, at], sems.at[8 + j]))
-    weight = pltpu.make_async_copy(w_out, held, sems.at[16])
-    for copy in blocks + [weight] + ends:
+    blocks = [
+        pltpu.make_async_copy(xs.at[j, 0:rows], x.at[:, 256 * j : 256 * (j + 1)], sems.at[j]) for j in range(8)
+    ]
+    weight = pltpu.make_async_copy(w_out, held, sems.at[8])
+    for copy in blocks:
         copy.start()
     sums = [0.0, 0.0, 0.0]
     for part in range(2):
         for copy in blocks[4 * part : 4 * (part + 1)]:
             copy.wait()
+        if part == 1:
+            weight.start()
         at = slice(1024 * part, 1024 * (part + 1))
         for i, w in enumerate((w_u, w_outer, w_inner)):
             sums[i] = sums[i] + jnp.dot(x[:, at], w[at], preferred_element_type=jnp.float32)
@@ -147,13 +146,6 @@
             target[32 * i : 32 * (i + 1)] = g[pl.ds(pl.multiple_of(HALO + 64 * i + 32 * which, 16), 32)]
     weight.wait()
     out_product(half[...], held, 1.0 / OUT_UP, sent)
-    alpha = (2.0 * LAYERS) ** 0.25
-    kept[:32] = alpha * f32(x[pl.ds(pl.multiple_of(HALO + 32 * tp, 16), 32)])
-    kept[32:] = alpha * f32(x[HALO - 8 : HALO])
-    for copy in ends:
-        copy.wait()
-    tail = f32(tails[...])
-    table[...] = tail[0:4] + tail[4:8] + tail[8:12]
 
 
 def front(xs, weights, taps):
@@ -161,24 +153,58 @@
     return pl.pallas_call(
         front_kernel,
         in_specs=[HBM, VMEM, VMEM, VMEM, HBM, VMEM],
-        out_specs=(VMEM,) * 4,
-        out_shape=(
-            shape((136, D), jnp.bfloat16),
-            shape((136, 256), jnp.bfloat16),
-            shape((40, D), jnp.float32),
-            shape((4, D), jnp.float32),
-        ),
+        out_specs=(VMEM,) * 2,
+        out_shape=(shape((136, D), jnp.bfloat16), shape((136, 256), jnp.bfloat16)),
         scratch_shapes=[
             pltpu.VMEM((HALO + 256, D), jnp.bfloat16),
-            pltpu.VMEM((16, D), jnp.bfloat16),
             pltpu.VMEM((HALO + 256, 256), jnp.bfloat16),
             pltpu.VMEM((136, 256), jnp.bfloat16),
             pltpu.VMEM((D, 256), jnp.bfloat16),
-            pltpu.SemaphoreType.DMA((17,)),
+            pltpu.SemaphoreType.DMA((9,)),
         ],
-        compiler_params=pltpu.CompilerParams(vmem_limit_bytes=49 * 2**20),
+        compiler_params=pltpu.CompilerParams(vmem_limit_bytes=50 * 2**20),
         cost_estimate=pl.CostEstimate(flops=1200000000, bytes_accessed=7000000, transcendentals=0),
     )(xs, *weights, taps)
+
+
+def aside_kernel(rows, w, xs, mine, kept, table, held, x, tails, sems):
+    tp = 2 * lax.axis_index("x") + lax.axis_index("core")
+    weight = pltpu.make_async_copy(w, held, sems.at[0])
+    weight.start()
+    copies = []
+    for j in range(8):
+        at = slice(256 * j, 256 * (j + 1))
+        start = pl.multiple_of(HALO + 32 * tp, 16)
+        copies.append(pltpu.make_async_copy(xs.at[j, pl.ds(start, 32)], x.at[0:32, at], sems.at[1 + j]))
+        copies.append(pltpu.make_async_copy(xs.at[j, HALO - 8 : HALO], x.at[32:40, at], sems.at[9 + j]))
+        copies.append(pltpu.make_async_copy(xs.at[j, HALO + 256 : HALO + 272], tails.at[:, at], sems.at[17 + j]))
+    for copy in copies:
+        copy.start()
+    weight.wait()
+    out_product(rows[...], held, 1.0 / OUT_UP, mine)
+    for copy in copies:
+        copy.wait()
+    kept[...] = (2.0 * LAYERS) ** 0.25 * f32(x[...])
+    tail = f32(tails[...])
+    table[...] = tail[0:4] + tail[4:8] + tail[8:12]
+
+
+def aside(rows, w, xs):
+    shape = jax.ShapeDtypeStruct
+    return pl.pallas_call(
+        aside_kernel,
+        in_specs=[VMEM, HBM, HBM],
+        out_specs=(VMEM,) * 3,
+        out_shape=(shape((136, D), jnp.bfloat16), shape((40, D), jnp.float32), shape((4, D), jnp.float32)),
+        scratch_shapes=[
+            pltpu.VMEM((D, 256), jnp.bfloat16),
+            pltpu.VMEM((40, D), jnp.bfloat16),
+            pltpu.VMEM((16, D), jnp.bfloat16),
+            pltpu.SemaphoreType.DMA((25,)),
+        ],
+        compiler_params=pltpu.CompilerParams(vmem_limit_bytes=52 * 2**20),
+        cost_estimate=pl.CostEstimate(flops=800000000, bytes_accessed=2000000, transcendentals=0),
+    )(rows, w, xs)
 
 
 def own_kernel(column, down, rows, w, mine, held, sem):

time: 165 us -> 165 us (level)
    pallas_call x0 -> x1, Pallas kernels: none -> 2.06 us  [aside(): pl.pallas_call(aside_kernel, in_specs=[VMEM, HBM, HBM], out_specs=(VMEM,)...]
  transfers between devices with their start and end apart: 5 -> 5, of which waited for: 1 -> 0; matrix products, arithmetic and copies ran while one was open for 2% -> 2% of each run, Pallas kernels for 4% -> 5%
where the time goes in v6:
time: 165 us; the launch traced here: 164 us
  blocking collectives  106 us (64%)
  starting transfers between devices  25.4 us (15%)
  Pallas kernels  14.4 us (9%)
  between operations  13.5 us (8%)
  other arithmetic  2.78 us (2%)
  local copies, waits for them, and re-layouts  2 us (1%)
    all_gather x1, blocking collectives, shards(): early = lax.all_gather(early.astype(jnp.float16), SP, axis=0, tiled=True)  55.5 us
    all_to_all x1, blocking collectives, shards(): got = lax.all_to_all(folded(got, mine), 'x', 0, 0, tiled=True)  15.3 us
    all_gather x1, blocking collectives, shards(): every = lax.all_gather(own.astype(jnp.float16), TP, axis=0, tiled=True)  15.1 us
    ppermute x2, starting transfers between devices, shards(): got = lax.ppermute(sent, 'core', [(0, 1), (1, 0)])  12.6 us
    all_to_all x1, blocking collectives, shards(): lax.all_to_all(bf(f32(got) + f32(mine)).reshape(4, 32, D), 'x', 0, 0, til...  11.5 us
    all_to_all x1, blocking collectives, shards(): lax.all_to_all(last(got, own, table), TP, 0, 0, tiled=True)  8.97 us
    all_to_all x1, starting transfers between devices, shards(): everyone = lax.all_to_all(copies, TP, 0, 0, tiled=True)  8.74 us
    ppermute x1, starting transfers between devices, shards(): halo = lax.ppermute(tokens[-HALO:], SP, [(i, i + 1) for i in range(63)])  4.01 us
  transfers between devices with their start and end apart: 5, of which 0 were waited for; matrix products, arithmetic and copies ran while one was open for 2% of the time, Pallas kernels for 5%

profile of v6, /device:TPU:1, one launch (start us, length us, event | category | flops | bytes accessed | tf_op | source)
XLA Modules:
  0.0 164.4 jit_solution(1991567470410930159)
XLA Ops:
  6.5 0.0 all-gather.4.cloned.1.call-start
  6.5 2.7 %shard_map.82 = (bf16[32,1024]{1,0:T(8,128)(2,1)}, bf16[32,1024]{1,0:T(8,128)(2,1)}, bf16[8,288,256]{2,1,0:T(8,128)(2,1)}) custom-call(bf16[2,32,256]{2,1,0:T(8,128)(2,1)} %value.1, bf16[2,32,256]{2,1,0:T(8,128)(2,1)} %outer.1, bf16[2,32,256]{2,1,0:T(8,128)(2,1)} %inner.1, bf16[2,32,256]{2,1,0:T(8,128)(2,1)} %bitcast.8, bf16[256,256]{1,0:T(8,128)(2,1)} %tokens.1, ...), custom_call_target="tpu_custom_call" | custom-call | flops 2000000 | bytes 1700000 | tf_op jit(solution)/shard_map/pallas_call | solution.py:66
  9.2 0.0 all-gather.4.cloned.1.call-update
  9.3 0.7 slice.15
  10.0 4.0 %collective-permute-start = (bf16[16,256]{1,0:T(8,128)(2,1)S(1)}, bf16[16,256]{1,0:T(8,128)(2,1)S(1)}, u32[]{:S(2)}, u32[]{:S(2)}) collective-permute-start(bf16[16,256]{1,0:T(8,128)(2,1)S(1)} %slice.15), channel_id=1, source_target_pairs={{0,8},{8,16},{16,24},{24,32},{32,40},{40,48},{48,56},{56,64},{64,7... | collective-permute-start | bytes 24584 | tf_op jit(solution)/shard_map/ppermute | solution.py:90
  14.0 0.9 convert_element_type.30
  14.8 0.0 collective-permute-done
  14.8 0.6 broadcast_dynamic-update-slice_fusion
  15.5 8.7 %all-to-all-start = ((bf16[8,288,256]{2,1,0:T(8,128)(2,1)}), bf16[8,288,256]{2,1,0:T(8,128)(2,1)}, u32[]{:S(2)}, u32[]{:S(2)}) async-start(bf16[8,288,256]{2,1,0:T(8,128)(2,1)} %broadcast_dynamic-update-slice_fusion), calls=%async_computation | async-start | bytes 2359296 | tf_op jit(solution)/shard_map/all_to_all | solution.py:94
  24.2 55.5 %all-gather.5 = f16[2048,1024]{1,0:T(8,128)(2,1)S(1)} all-gather(f16[32,1024]{1,0:T(8,128)(2,1)S(1)} %convert_element_type.30), channel_id=1, replica_groups=mesh['z'=8,'y'=8,'x'=4,'core'=2] {'z','y'}, dimensions={0}, use_global_device_ids=true | all-gather | bytes 4259840 | tf_op jit(solution)/shard_map/all_gather | solution.py:95
  79.7 1.6 slice_convert_fusion
  81.3 0.0 all-to-all-done.xs
  81.3 0.0 copy-done
  81.3 3.5 %shard_map.83 = (bf16[136,2048]{1,0:T(8,128)(2,1)S(1)}, bf16[136,256]{1,0:T(8,128)(2,1)S(1)}) custom-call(bf16[8,288,256]{2,1,0:T(8,128)(2,1)} %all-to-all-done.xs, bf16[2048,256]{1,0:T(8,128)(2,1)S(1)} %get-tuple-element.32.w_u, bf16[2048,256]{1,0:T(8,128)(2,1)S(1)} %get-tuple-element.31.w_outer, bf16[2048,256]{1,0:T(8,128)(2,1)S(1)} %get-tuple-element.30.w_inner, ...), custom_call_target="tpu_custom_call" | custom-call | flops 1200000000 | bytes 7000000 | tf_op jit(solution)/shard_map/pallas_call | solution.py:153
  84.9 10.6 %collective-permute-start.1 = (bf16[136,2048]{1,0:T(8,128)(2,1)S(1)}, bf16[136,2048]{1,0:T(8,128)(2,1)S(1)}, u32[]{:S(2)}, u32[]{:S(2)}) collective-permute-start(bf16[136,2048]{1,0:T(8,128)(2,1)S(1)} %get-tuple-element.19), channel_id=1, source_target_pairs={{0,1},{1,0},{2,3},{3,2},{4,5},{5,4},{6,7},{7,6},{8,9},{9,8},{10,11... | collective-permute-start | bytes 1671176 | tf_op jit(solution)/shard_map/ppermute | solution.py:99
  95.5 2.1 %shard_map.84 = (bf16[136,2048]{1,0:T(8,128)(2,1)S(1)}, f32[40,2048]{1,0:T(8,128)S(1)}, f32[4,2048]{1,0:T(4,128)S(1)}) custom-call(bf16[136,256]{1,0:T(8,128)(2,1)S(1)} %get-tuple-element.20.rows, bf16[2048,256]{1,0:T(8,128)(2,1)} %get-tuple-element.29.w_out.w, bf16[8,288,256]{2,1,0:T(8,128)(2,1)} %all-to-all-done.xs), custom_call_target="tpu_custom_call" | custom-call | flops 800000000 | bytes 2000000 | tf_op jit(solution)/shard_map/pallas_call | solution.py:194
  97.5 0.0 collective-permute-done.1.got
  97.5 0.3 shard_map.85
  97.8 15.3 %all_to_all.20.got = bf16[4,32,2176]{2,1,0:T(8,128)(2,1)S(1)} all-to-all(bf16[4,32,2176]{2,1,0:T(8,128)(2,1)S(1)} %shard_map.85), channel_id=1, replica_groups=mesh['z'=8,'y'=8,'x'=4,'core'=2] {'x'}, dimensions={0} | all-to-all | bytes 1114112 | tf_op jit(solution)/shard_map/all_to_all | solution.py:101
  113.1 0.3 shard_map.86
  113.4 15.1 %all-gather.6 = f16[256,2048]{1,0:T(8,128)(2,1)S(1)} all-gather(f16[32,2048]{1,0:T(8,128)(2,1)S(1)} %convert_element_type.35), channel_id=1, replica_groups=mesh['z'=8,'y'=8,'x'=4,'core'=2] {'x','core'}, dimensions={0}, use_global_device_ids=true | all-gather | bytes 1179648 | tf_op jit(solution)/shard_map/all_gather | solution.py:103
  128.5 0.1 convert_element_type.36.x
  128.7 0.0 all-gather.4.cloned.1.call-done.w
  128.7 3.5 %shard_map.87 = (bf16[128,2048]{1,0:T(8,128)(2,1)S(1)}, bf16[128,256]{1,0:T(8,128)(2,1)S(1)}) custom-call(bf16[256,2048]{1,0:T(8,128)(2,1)S(1)} %convert_element_type.36.x, bf16[8,2048]{1,0:T(8,128)(2,1)S(1)} %get-tuple-element.25.before, bf16[2048,1024]{1,0:T(8,128)(2,1)} %all-gather.4.cloned.1.call-done.w, f32[3,2,256]{2,1,0:T(2,128)S(1)} %bitcast.5), custom_call_target="tpu_custom_call" | custom-call | flops 1200000000 | bytes 7000000 | tf_op jit(solution)/shard_map/pallas_call | solution.py:303
  132.2 2.1 %collective-permute-start.2 = (bf16[128,2048]{1,0:T(8,128)(2,1)S(1)}, bf16[128,2048]{1,0:T(8,128)(2,1)S(1)}, u32[]{:S(2)}, u32[]{:S(2)}) collective-permute-start(bf16[128,2048]{1,0:T(8,128)(2,1)S(1)} %get-tuple-element.27), channel_id=1, source_target_pairs={{0,1},{1,0},{2,3},{3,2},{4,5},{5,4},{6,7},{7,6},{8,9},{9,8},{10,11... | collective-permute-start | bytes 1572872 | tf_op jit(solution)/shard_map/ppermute | solution.py:106
  134.3 1.7 %shard_map.88 = bf16[128,2048]{1,0:T(8,128)(2,1)S(1)} custom-call(bf16[128,256]{1,0:T(8,128)(2,1)S(1)} %get-tuple-element.28.rows, bf16[2048,1024]{1,0:T(8,128)(2,1)} %all-gather.4.cloned.1.call-done.w), custom_call_target="tpu_custom_call" | custom-call | flops 800000000 | bytes 2000000 | tf_op jit(solution)/shard_map/pallas_call | solution.py:218
  136.0 0.0 collective-permute-done.2
  136.0 0.1 add_convert_fusion
  136.1 11.5 %all_to_all.21.got = bf16[4,32,2048]{2,1,0:T(8,128)(2,1)S(1)} all-to-all(bf16[4,32,2048]{2,1,0:T(8,128)(2,1)S(1)} %bitcast.6), channel_id=1, replica_groups=mesh['z'=8,'y'=8,'x'=4,'core'=2] {'x'}, dimensions={0} | all-to-all | bytes 1048576 | tf_op jit(solution)/shard_map/all_to_all | solution.py:108
  147.6 0.3 shard_map.89
  147.9 9.0 %all_to_all.22 = bf16[8,32,256]{2,1,0:T(8,128)(2,1)S(1)} all-to-all(bf16[8,32,256]{2,1,0:T(8,128)(2,1)S(1)} %shard_map.89), channel_id=1, replica_groups=mesh['z'=8,'y'=8,'x'=4,'core'=2] {'x','core'}, dimensions={0} | all-to-all | bytes 262144 | tf_op jit(solution)/shard_map/all_to_all | solution.py:109
  156.9 0.7 copy.11
  (2 shorter events, 0.0 us)
Async XLA Ops:
  6.5 122.1 %all-gather.4.cloned.1.call-start = ((), (), s32[]{:S(2)}) async-start(), calls=%async_computation.4 | async-start | bytes 4259840 | tf_op jit(solution)/shard_map/all_gather | solution.py:92
  10.0 4.9 %collective-permute-start = (bf16[16,256]{1,0:T(8,128)(2,1)S(1)}, bf16[16,256]{1,0:T(8,128)(2,1)S(1)}, u32[]{:S(2)}, u32[]{:S(2)}) collective-permute-start(bf16[16,256]{1,0:T(8,128)(2,1)S(1)} %slice.15), channel_id=1, source_target_pairs={{0,8},{8,16},{16,24},{24,32},{32,40},{40,48},{48,56},{56,64},{64,7... | collective-permute-start | bytes 24584 | tf_op jit(solution)/shard_map/ppermute | solution.py:90
  15.5 65.8 %all-to-all-start = ((bf16[8,288,256]{2,1,0:T(8,128)(2,1)}), bf16[8,288,256]{2,1,0:T(8,128)(2,1)}, u32[]{:S(2)}, u32[]{:S(2)}) async-start(bf16[8,288,256]{2,1,0:T(8,128)(2,1)} %broadcast_dynamic-update-slice_fusion), calls=%async_computation | async-start | bytes 2359296 | tf_op jit(solution)/shard_map/all_to_all | solution.py:94
  79.7 1.6 %copy-start = (f32[2,3,256]{2,0,1:T(2,128)S(1)}, f32[2,3,256]{2,0,1:T(2,128)}, u32[]{:S(2)}) copy-start(f32[2,3,256]{2,0,1:T(2,128)} %param.12) | copy-start | bytes 18436
  84.9 12.7 %collective-permute-start.1 = (bf16[136,2048]{1,0:T(8,128)(2,1)S(1)}, bf16[136,2048]{1,0:T(8,128)(2,1)S(1)}, u32[]{:S(2)}, u32[]{:S(2)}) collective-permute-start(bf16[136,2048]{1,0:T(8,128)(2,1)S(1)} %get-tuple-element.19), channel_id=1, source_target_pairs={{0,1},{1,0},{2,3},{3,2},{4,5},{5,4},{6,7},{7,6},{8,9},{9,8},{10,11... | collective-permute-start | bytes 1671176 | tf_op jit(solution)/shard_map/ppermute | solution.py:99
  132.2 3.8 %collective-permute-start.2 = (bf16[128,2048]{1,0:T(8,128)(2,1)S(1)}, bf16[128,2048]{1,0:T(8,128)(2,1)S(1)}, u32[]{:S(2)}, u32[]{:S(2)}) collective-permute-start(bf16[128,2048]{1,0:T(8,128)(2,1)S(1)} %get-tuple-element.27), channel_id=1, source_target_pairs={{0,1},{1,0},{2,3},{3,2},{4,5},{5,4},{6,7},{7,6},{8,9},{9,8},{10,11... | collective-permute-start | bytes 1572872 | tf_op jit(solution)/shard_map/ppermute | solution.py:106
Sparse Core Ops, SparseCore 0:
  10.4 91.4 all-gather.3

commit v7 on v6

--- a/solution.py
+++ b/solution.py
@@ -1,5 +1,3 @@
-import functools
-
 import jax
 import jax.numpy as jnp
 from jax import lax
@@ -102,11 +100,12 @@
     own, before = middle(got, kept, table)
     every = lax.all_gather(own.astype(jnp.float16), TP, axis=0, tiled=True)
 
-    sent, half = rear(bf(every), before, late, taps)
+    sent, gated, resid = rear(bf(every), before, late, taps)
     got = lax.ppermute(sent, "core", [(0, 1), (1, 0)])
-    mine = own_product(half, late, 768, 1.0, 52)
-    got = lax.all_to_all(bf(f32(got) + f32(mine)).reshape(4, 32, D), "x", 0, 0, tiled=True)
-    return lax.all_to_all(last(got, own, table), TP, 0, 0, tiled=True).reshape(256, 256)
+    mine = own_product(gated, late)
+    got = lax.all_to_all(bf(f32(got) + f32(mine)), "x", 0, 0, tiled=True)
+    pre, stats = moments(got, resid)
+    return last(lax.all_to_all(stats, TP, 0, 0, tiled=True), pre, gain, bias)
 
 
 def out_product(rows, w_out, down, target):
@@ -207,25 +206,6 @@
     )(rows, w, xs)
 
 
-def own_kernel(column, down, rows, w, mine, held, sem):
-    copy = pltpu.make_async_copy(w.at[:, column : column + 256], held, sem.at[0])
-    copy.start()
-    copy.wait()
-    out_product(rows[...], held, down, mine)
-
-
-def own_product(rows, w, column, down, limit):
-    return pl.pallas_call(
-        functools.partial(own_kernel, column, down),
-        in_specs=[VMEM, HBM],
-        out_specs=VMEM,
-        out_shape=jax.ShapeDtypeStruct((rows.shape[0], D), jnp.bfloat16),
-        scratch_shapes=[pltpu.VMEM((D, 256), jnp.bfloat16), pltpu.SemaphoreType.DMA((1,))],
-        compiler_params=pltpu.CompilerParams(vmem_limit_bytes=limit * 2**20),
-        cost_estimate=pl.CostEstimate(flops=800000000, bytes_accessed=2000000, transcendentals=0),
-    )(rows, w)
-
-
 def fold_kernel(got, mine, out, strip):
     total = f32(got[...]) + f32(mine[...])
     for i in range(4):
@@ -269,33 +249,40 @@
     )(got, kept, table)
 
 
-def rear_kernel(x, before, w, taps, sent, own, held, acc, g, half, sems):
+def rear_kernel(x, before, w, taps, sent, g, resid, held, other, acc, sems):
     core = lax.axis_index("core")
+    tp = 2 * lax.axis_index("x") + core
     first = jnp.logical_and(lax.axis_index("z") == 0, lax.axis_index("y") == 0)
     step = D // 4
     copies = [
-        pltpu.make_async_copy(w.at[at, 0:768], held.at[at, 0:768], sems.at[i])
+        pltpu.make_async_copy(w.at[at, 0:768], held.at[at], sems.at[i])
         for i, at in enumerate(pl.ds(step * i, step) for i in range(4))
     ]
-    copies.append(pltpu.make_async_copy(w.at[:, 768:1024], held.at[:, 768:1024], sems.at[4]))
+    for i in range(4):
+        start = pl.multiple_of(256 * (2 * i + 1 - core), 256)
+        copies.append(pltpu.make_async_copy(w.at[pl.ds(start, 256), 768:1024], other.at[i], sems.at[4 + i]))
     for copy in copies:
         copy.start()
+    alpha = (2.0 * LAYERS) ** 0.25
+    resid[...] = alpha * f32(x[:, pl.ds(pl.multiple_of(256 * tp, 256), 256)])
     for i in range(4):
         copies[i].wait()
         at = slice(step * i, step * (i + 1))
         for rows, source in ((slice(0, 8), before), (slice(8, 264), x)):
-            part = jnp.dot(source[:, at], held[at, :768], preferred_element_type=jnp.float32)
+            part = jnp.dot(source[:, at], held[at], preferred_element_type=jnp.float32)
             acc[rows] = part if i == 0 else acc[rows] + part
     u, outer, inner = (f32(bf(acc[:, 256 * i : 256 * (i + 1)])) for i in range(3))
     row = lax.broadcasted_iota(jnp.int32, u.shape, 0)
     z = jnp.where(jnp.logical_and(first, row < 8), 0.0, inner * u)
     conv = taps[2, 1:2] * z + taps[1, 1:2] * pltpu.roll(z, 1, 0) + taps[0, 1:2] * pltpu.roll(z, 2, 0)
     g[...] = bf((outer * conv)[8:])
-    for target, which in ((half, 1 - core), (own, core)):
-        for i in range(4):
-            target[32 * i : 32 * (i + 1)] = g[pl.ds(pl.multiple_of(64 * i + 32 * which, 16), 32)]
-    copies[4].wait()
-    out_product(half[...], held.at[:, 768:1024], 1.0, sent)
+    for i in range(4):
+        copies[4 + i].wait()
+        sent[i] = bf(times_turned(g[...], other[i]))
+
+
+def times_turned(a, b):
+    return lax.dot_general(a, b, (((1,), (1,)), ((), ())), preferred_element_type=jnp.float32)
 
 
 def rear(x, before, w, taps):
@@ -303,35 +290,90 @@
     return pl.pallas_call(
         rear_kernel,
         in_specs=[VMEM, VMEM, HBM, VMEM],
-        out_specs=(VMEM, VMEM),
-        out_shape=(shape((128, D), jnp.bfloat16), shape((128, 256), jnp.bfloat16)),
+        out_specs=(VMEM,) * 3,
+        out_shape=(
+            shape((4, 256, 256), jnp.bfloat16),
+            shape((256, 256), jnp.bfloat16),
+            shape((256, 256), jnp.float32),
+        ),
         scratch_shapes=[
-            pltpu.VMEM((D, 1024), jnp.bfloat16),
+            pltpu.VMEM((D, 768), jnp.bfloat16),
+            pltpu.VMEM((4, 256, 256), jnp.bfloat16),
             pltpu.VMEM((264, 768), jnp.float32),
-            pltpu.VMEM((256, 256), jnp.bfloat16),
-            pltpu.VMEM((128, 256), jnp.bfloat16),
-            pltpu.SemaphoreType.DMA((5,)),
+            pltpu.SemaphoreType.DMA((8,)),
         ],
         compiler_params=pltpu.CompilerParams(vmem_limit_bytes=50 * 2**20),
         cost_estimate=pl.CostEstimate(flops=1200000000, bytes_accessed=7000000, transcendentals=0),
     )(x, before, w, taps)
 
 
-def last_kernel(got, own, table, out):
-    total = f32(got[0]) + f32(got[1]) + f32(got[2]) + f32(got[3])
-    alpha = (2.0 * LAYERS) ** 0.25
-    state = norm(alpha * f32(own[...]) + total, table[1:2], table[3:4])
+def own_kernel(g, w, mine, held, sems):
+    core = lax.axis_index("core")
+    copies = []
+    for i in range(4):
+        start = pl.multiple_of(256 * (2 * i + core), 256)
+        copies.append(pltpu.make_async_copy(w.at[pl.ds(start, 256), 768:1024], held.at[i], sems.at[i]))
+    for copy in copies:
+        copy.start()
+    for i in range(4):
+        copies[i].wait()
+        mine[i] = bf(times_turned(g[...], held[i]))
+
+
+def own_product(g, w):
+    return pl.pallas_call(
+        own_kernel,
+        in_specs=[VMEM, HBM],
+        out_specs=VMEM,
+        out_shape=jax.ShapeDtypeStruct((4, 256, 256), jnp.bfloat16),
+        scratch_shapes=[pltpu.VMEM((4, 256, 256), jnp.bfloat16), pltpu.SemaphoreType.DMA((4,))],
+        compiler_params=pltpu.CompilerParams(vmem_limit_bytes=52 * 2**20),
+        cost_estimate=pl.CostEstimate(flops=800000000, bytes_accessed=2000000, transcendentals=0),
+    )(g, w)
+
+
+def moment_kernel(got, resid, pre, stats):
+    total = resid[...] + f32(got[0]) + f32(got[1]) + f32(got[2]) + f32(got[3])
+    pre[...] = total
+    ones = jnp.ones((8, 256), jnp.float32)
+    along = lambda v: lax.dot_general(
+        ones, v, (((1,), (1,)), ((), ())), precision=lax.Precision.HIGHEST, preferred_element_type=jnp.float32
+    )
+    cent = total - jnp.mean(total, axis=-1, keepdims=True)
+    row = lax.broadcasted_iota(jnp.int32, (8, 256), 0)
+    both = jnp.where(row == 0, along(total) * (1.0 / 256), along(cent * cent))
     for i in range(8):
-        out[i] = state[:, 256 * i : 256 * (i + 1)]
-
-
-def last(got, own, table):
-    return pl.pallas_call(
-        last_kernel,
-        out_shape=jax.ShapeDtypeStruct((8, 32, 256), jnp.bfloat16),
+        stats[i] = both
+
+
+def moments(got, resid):
+    shape = jax.ShapeDtypeStruct
+    return pl.pallas_call(
+        moment_kernel,
+        out_shape=(shape((256, 256), jnp.float32), shape((8, 8, 256), jnp.float32)),
         compiler_params=pltpu.CompilerParams(vmem_limit_bytes=6 * 2**20),
         cost_estimate=pl.CostEstimate(flops=2000000, bytes_accessed=1200000, transcendentals=100),
-    )(got, own, table)
+    )(got, resid)
+
+
+def last_kernel(stats, pre, gain, bias, out):
+    means = jnp.concatenate([stats[i, 0:1] for i in range(8)], axis=0)
+    spread = jnp.concatenate([stats[i, 1:2] for i in range(8)], axis=0)
+    mean = jnp.mean(means, axis=0, keepdims=True)
+    off = means - mean
+    var = (jnp.sum(spread, axis=0, keepdims=True) + 256.0 * jnp.sum(off * off, axis=0, keepdims=True)) * (1.0 / D)
+    turned = lambda v: jnp.concatenate([jnp.transpose(jnp.broadcast_to(v, (128, 256)))] * 2, axis=1)
+    state = (pre[...] - turned(mean)) * turned(lax.rsqrt(var + 1e-05))
+    out[...] = bf(state * gain[1:2] + bias[1:2])
+
+
+def last(stats, pre, gain, bias):
+    return pl.pallas_call(
+        last_kernel,
+        out_shape=jax.ShapeDtypeStruct((256, 256), jnp.bfloat16),
+        compiler_params=pltpu.CompilerParams(vmem_limit_bytes=6 * 2**20),
+        cost_estimate=pl.CostEstimate(flops=2000000, bytes_accessed=1200000, transcendentals=100),
+    )(stats, pre, gain, bias)
 
 
 def solution(mesh):

time: 165 us -> 166 us (level)
  Pallas kernels: 14.4 us -> 16.2 us
    pallas_call x2 -> x3, Pallas kernels: 2.01 us -> 3.39 us  [the longest x1 1.95 us: own_product(): pl.pallas_call(own_kernel, in_specs=[VMEM, HBM], out_specs=VMEM, out_shap...]
where the time goes in v7:
time: 166 us; the launch traced here: 165 us
  blocking collectives  106 us (64%)
  starting transfers between devices  25.5 us (15%)
  Pallas kernels  16.2 us (10%)
  between operations  13.5 us (8%)
  other arithmetic  2.78 us (2%)
    all_gather x1, blocking collectives, shards(): early = lax.all_gather(early.astype(jnp.float16), SP, axis=0, tiled=True)  55.3 us
    all_to_all x1, blocking collectives, shards(): got = lax.all_to_all(folded(got, mine), 'x', 0, 0, tiled=True)  15.4 us
    all_gather x1, blocking collectives, shards(): every = lax.all_gather(own.astype(jnp.float16), TP, axis=0, tiled=True)  15.1 us
    ppermute x2, starting transfers between devices, shards(): got = lax.ppermute(sent, 'core', [(0, 1), (1, 0)])  12.7 us
    all_to_all x1, blocking collectives, shards(): got = lax.all_to_all(bf(f32(got) + f32(mine)), 'x', 0, 0, tiled=True)  11.5 us
    all_to_all x1, starting transfers between devices, shards(): everyone = lax.all_to_all(copies, TP, 0, 0, tiled=True)  8.74 us
    all_to_all x1, blocking collectives, shards(): return last(lax.all_to_all(stats, TP, 0, 0, tiled=True), pre, gain, bias)  8.58 us
    ppermute x1, starting transfers between devices, shards(): halo = lax.ppermute(tokens[-HALO:], SP, [(i, i + 1) for i in range(63)])  4.01 us
  transfers between devices with their start and end apart: 5, of which 0 were waited for; matrix products, arithmetic and copies ran while one was open for 2% of the time, Pallas kernels for 5%

profile of v7, /device:TPU:1, one launch (start us, length us, event | category | flops | bytes accessed | tf_op | source)
XLA Modules:
  0.0 165.4 jit_solution(12170727189251424392)
XLA Ops:
  6.5 2.8 %shard_map.82 = (bf16[32,1024]{1,0:T(8,128)(2,1)}, bf16[32,1024]{1,0:T(8,128)(2,1)}, bf16[8,288,256]{2,1,0:T(8,128)(2,1)}) custom-call(bf16[2,32,256]{2,1,0:T(8,128)(2,1)} %value.1, bf16[2,32,256]{2,1,0:T(8,128)(2,1)} %outer.1, bf16[2,32,256]{2,1,0:T(8,128)(2,1)} %inner.1, bf16[2,32,256]{2,1,0:T(8,128)(2,1)} %bitcast.4, bf16[256,256]{1,0:T(8,128)(2,1)} %tokens.1, ...), custom_call_target="tpu_custom_call" | custom-call | flops 2000000 | bytes 1700000 | tf_op jit(solution)/shard_map/pallas_call | solution.py:64
  9.3 0.0 all-gather.4.cloned.1.call-update
  9.3 0.7 slice.15
  10.0 4.0 %collective-permute-start = (bf16[16,256]{1,0:T(8,128)(2,1)S(1)}, bf16[16,256]{1,0:T(8,128)(2,1)S(1)}, u32[]{:S(2)}, u32[]{:S(2)}) collective-permute-start(bf16[16,256]{1,0:T(8,128)(2,1)S(1)} %slice.15), channel_id=1, source_target_pairs={{0,8},{8,16},{16,24},{24,32},{32,40},{40,48},{48,56},{56,64},{64,7... | collective-permute-start | bytes 24584 | tf_op jit(solution)/shard_map/ppermute | solution.py:88
  14.0 0.9 convert_element_type.30
  14.9 0.0 collective-permute-done
  14.9 0.6 broadcast_dynamic-update-slice_fusion
  15.5 8.7 %all-to-all-start = ((bf16[8,288,256]{2,1,0:T(8,128)(2,1)}), bf16[8,288,256]{2,1,0:T(8,128)(2,1)}, u32[]{:S(2)}, u32[]{:S(2)}) async-start(bf16[8,288,256]{2,1,0:T(8,128)(2,1)} %broadcast_dynamic-update-slice_fusion), calls=%async_computation | async-start | bytes 2359296 | tf_op jit(solution)/shard_map/all_to_all | solution.py:92
  24.3 55.3 %all-gather.5 = f16[2048,1024]{1,0:T(8,128)(2,1)S(1)} all-gather(f16[32,1024]{1,0:T(8,128)(2,1)S(1)} %convert_element_type.30), channel_id=1, replica_groups=mesh['z'=8,'y'=8,'x'=4,'core'=2] {'z','y'}, dimensions={0}, use_global_device_ids=true | all-gather | bytes 4259840 | tf_op jit(solution)/shard_map/all_gather | solution.py:93
  79.6 1.6 slice_convert_fusion
  81.3 0.0 all-to-all-done.xs
  81.3 3.5 %shard_map.83 = (bf16[136,2048]{1,0:T(8,128)(2,1)S(1)}, bf16[136,256]{1,0:T(8,128)(2,1)S(1)}) custom-call(bf16[8,288,256]{2,1,0:T(8,128)(2,1)} %all-to-all-done.xs, bf16[2048,256]{1,0:T(8,128)(2,1)S(1)} %get-tuple-element.38.w_u, bf16[2048,256]{1,0:T(8,128)(2,1)S(1)} %get-tuple-element.37.w_outer, bf16[2048,256]{1,0:T(8,128)(2,1)S(1)} %get-tuple-element.36.w_inner, ...), custom_call_target="tpu_custom_call" | custom-call | flops 1200000000 | bytes 7000000 | tf_op jit(solution)/shard_map/pallas_call | solution.py:152
  84.8 10.7 %collective-permute-start.1 = (bf16[136,2048]{1,0:T(8,128)(2,1)S(1)}, bf16[136,2048]{1,0:T(8,128)(2,1)S(1)}, u32[]{:S(2)}, u32[]{:S(2)}) collective-permute-start(bf16[136,2048]{1,0:T(8,128)(2,1)S(1)} %get-tuple-element.22), channel_id=1, source_target_pairs={{0,1},{1,0},{2,3},{3,2},{4,5},{5,4},{6,7},{7,6},{8,9},{9,8},{10,11... | collective-permute-start | bytes 1671176 | tf_op jit(solution)/shard_map/ppermute | solution.py:97
  95.5 2.1 %shard_map.84 = (bf16[136,2048]{1,0:T(8,128)(2,1)S(1)}, f32[40,2048]{1,0:T(8,128)S(1)}, f32[4,2048]{1,0:T(4,128)S(1)}) custom-call(bf16[136,256]{1,0:T(8,128)(2,1)S(1)} %get-tuple-element.23.rows, bf16[2048,256]{1,0:T(8,128)(2,1)} %get-tuple-element.35.w_out.w, bf16[8,288,256]{2,1,0:T(8,128)(2,1)} %all-to-all-done.xs), custom_call_target="tpu_custom_call" | custom-call | flops 800000000 | bytes 2000000 | tf_op jit(solution)/shard_map/pallas_call | solution.py:193
  97.6 0.0 collective-permute-done.1.got
  97.6 0.3 shard_map.85
  97.9 15.4 %all_to_all.20.got = bf16[4,32,2176]{2,1,0:T(8,128)(2,1)S(1)} all-to-all(bf16[4,32,2176]{2,1,0:T(8,128)(2,1)S(1)} %shard_map.85), channel_id=1, replica_groups=mesh['z'=8,'y'=8,'x'=4,'core'=2] {'x'}, dimensions={0} | all-to-all | bytes 1114112 | tf_op jit(solution)/shard_map/all_to_all | solution.py:99
  113.3 0.3 shard_map.86
  113.6 15.1 %all-gather.6 = f16[256,2048]{1,0:T(8,128)(2,1)S(1)} all-gather(f16[32,2048]{1,0:T(8,128)(2,1)S(1)} %convert_element_type.35), channel_id=1, replica_groups=mesh['z'=8,'y'=8,'x'=4,'core'=2] {'x','core'}, dimensions={0}, use_global_device_ids=true | all-gather | bytes 1179648 | tf_op jit(solution)/shard_map/all_gather | solution.py:101
  128.7 0.1 convert_element_type.36.x
  128.9 0.0 all-gather.4.cloned.1.call-done.w
  128.9 3.9 %shard_map.87 = (bf16[4,256,256]{2,1,0:T(8,128)(2,1)S(1)}, bf16[256,256]{1,0:T(8,128)(2,1)S(1)}, f32[256,256]{1,0:T(8,128)S(1)}) custom-call(bf16[256,2048]{1,0:T(8,128)(2,1)S(1)} %convert_element_type.36.x, bf16[8,2048]{1,0:T(8,128)(2,1)S(1)} %get-tuple-element.28.before, bf16[2048,1024]{1,0:T(8,128)(2,1)} %all-gather.4.cloned.1.call-done.w, ...), custom_call_target="tpu_custom_call" | custom-call | flops 1200000000 | bytes 7000000 | tf_op jit(solution)/shard_map/pallas_call | solution.py:290
  132.8 2.1 %collective-permute-start.2 = (bf16[4,256,256]{2,1,0:T(8,128)(2,1)S(1)}, bf16[4,256,256]{2,1,0:T(8,128)(2,1)S(1)}, u32[]{:S(2)}, u32[]{:S(2)}) collective-permute-start(bf16[4,256,256]{2,1,0:T(8,128)(2,1)S(1)} %get-tuple-element.30), channel_id=1, source_target_pairs={{0,1},{1,0},{2,3},{3,2},{4,5},{5,4},{6,7},{7,6},{8,9},{9,8},{10,11... | collective-permute-start | bytes 1572872 | tf_op jit(solution)/shard_map/ppermute | solution.py:104
  134.9 2.0 %shard_map.88 = bf16[4,256,256]{2,1,0:T(8,128)(2,1)S(1)} custom-call(bf16[256,256]{1,0:T(8,128)(2,1)S(1)} %get-tuple-element.31.g, bf16[2048,1024]{1,0:T(8,128)(2,1)} %all-gather.4.cloned.1.call-done.w), custom_call_target="tpu_custom_call" | custom-call | flops 800000000 | bytes 2000000 | tf_op jit(solution)/shard_map/pallas_call | solution.py:324
  136.8 0.0 collective-permute-done.2
  136.8 0.1 add_convert_fusion
  137.0 0.0 copy-start.1
  137.0 0.0 copy-start.2
  137.0 11.5 %all_to_all.21.got = bf16[4,256,256]{2,1,0:T(8,128)(2,1)S(1)} all-to-all(bf16[4,256,256]{2,1,0:T(8,128)(2,1)S(1)} %add_convert_fusion), channel_id=1, replica_groups=mesh['z'=8,'y'=8,'x'=4,'core'=2] {'x'}, dimensions={0} | all-to-all | bytes 1048576 | tf_op jit(solution)/shard_map/all_to_all | solution.py:106
  148.5 0.6 shard_map.89
  149.1 8.6 %all_to_all.22.stats = f32[8,8,256]{2,1,0:T(8,128)S(1)} all-to-all(f32[8,8,256]{2,1,0:T(8,128)S(1)} %get-tuple-element.33), channel_id=1, replica_groups=mesh['z'=8,'y'=8,'x'=4,'core'=2] {'x','core'}, dimensions={0} | all-to-all | bytes 131072 | tf_op jit(solution)/shard_map/all_to_all | solution.py:108
  157.7 0.8 shard_map.90
  (6 shorter events, 0.0 us)
Async XLA Ops:
  6.5 122.3 %all-gather.4.cloned.1.call-start = ((), (), s32[]{:S(2)}) async-start(), calls=%async_computation.4 | async-start | bytes 4259840 | tf_op jit(solution)/shard_map/all_gather | solution.py:90
  10.0 4.9 %collective-permute-start = (bf16[16,256]{1,0:T(8,128)(2,1)S(1)}, bf16[16,256]{1,0:T(8,128)(2,1)S(1)}, u32[]{:S(2)}, u32[]{:S(2)}) collective-permute-start(bf16[16,256]{1,0:T(8,128)(2,1)S(1)} %slice.15), channel_id=1, source_target_pairs={{0,8},{8,16},{16,24},{24,32},{32,40},{40,48},{48,56},{56,64},{64,7... | collective-permute-start | bytes 24584 | tf_op jit(solution)/shard_map/ppermute | solution.py:88
  15.5 65.7 %all-to-all-start = ((bf16[8,288,256]{2,1,0:T(8,128)(2,1)}), bf16[8,288,256]{2,1,0:T(8,128)(2,1)}, u32[]{:S(2)}, u32[]{:S(2)}) async-start(bf16[8,288,256]{2,1,0:T(8,128)(2,1)} %broadcast_dynamic-update-slice_fusion), calls=%async_computation | async-start | bytes 2359296 | tf_op jit(solution)/shard_map/all_to_all | solution.py:92
  79.6 1.6 copy-start
  84.8 12.7 %collective-permute-start.1 = (bf16[136,2048]{1,0:T(8,128)(2,1)S(1)}, bf16[136,2048]{1,0:T(8,128)(2,1)S(1)}, u32[]{:S(2)}, u32[]{:S(2)}) collective-permute-start(bf16[136,2048]{1,0:T(8,128)(2,1)S(1)} %get-tuple-element.22), channel_id=1, source_target_pairs={{0,1},{1,0},{2,3},{3,2},{4,5},{5,4},{6,7},{7,6},{8,9},{9,8},{10,11... | collective-permute-start | bytes 1671176 | tf_op jit(solution)/shard_map/ppermute | solution.py:97
  132.8 4.0 %collective-permute-start.2 = (bf16[4,256,256]{2,1,0:T(8,128)(2,1)S(1)}, bf16[4,256,256]{2,1,0:T(8,128)(2,1)S(1)}, u32[]{:S(2)}, u32[]{:S(2)}) collective-permute-start(bf16[4,256,256]{2,1,0:T(8,128)(2,1)S(1)} %get-tuple-element.30), channel_id=1, source_target_pairs={{0,1},{1,0},{2,3},{3,2},{4,5},{5,4},{6,7},{7,6},{8,9},{9,8},{10,11... | collective-permute-start | bytes 1572872 | tf_op jit(solution)/shard_map/ppermute | solution.py:104
  137.0 20.7 %copy-start.1 = (f32[2,256]{1,0:T(2,128)S(1)}, f32[2,256]{1,0:T(2,128)}, u32[]{:S(2)}) copy-start(f32[2,256]{1,0:T(2,128)} %gain.3) | copy-start | bytes 6148
  137.0 20.7 %copy-start.2 = (f32[2,256]{1,0:T(2,128)S(1)}, f32[2,256]{1,0:T(2,128)}, u32[]{:S(2)}) copy-start(f32[2,256]{1,0:T(2,128)} %bias.3) | copy-start | bytes 6148
Sparse Core Ops, SparseCore 0:
  10.4 91.6 all-gather.3
